TPU v7x, 32 devices: a whole 2x2x4 slice. The times are simulated.
32 devices in a mesh: grp: 2 (over y), tp: 4 (over z), dp: 4 (over x, core).
Axes of the slice: x: 2, y: 2, z: 4, core: 2. Of those that a mesh axis runs over, the one named last changes fastest.
Arguments:
- residual_slot_vectors: bfloat16 [128, 4, 4096], P('grp', None, 'dp'), parts along dimension 0, may hold values from -25 to 25
- active_counts: int32 [128], P(('grp', 'dp')), parts along dimension 0, may hold values from 1 to 4, 96 in all
- lookup_map: bfloat16 [2, 4096, 4096], P(None, 'dp', 'tp'), may hold values from -0.09375 to 0.09375
- address_map: bfloat16 [2, 4096, 4096], P(None, 'dp', 'tp'), may hold values from -0.09375 to 0.09375
- content_map: bfloat16 [2, 4096, 4096], P(None, 'dp', 'tp'), may hold values from -0.09375 to 0.09375
- result_valve_map: bfloat16 [2, 4096, 4096], P(None, 'dp', 'tp'), may hold values from -0.09375 to 0.09375
- fading_map_coefficients: bfloat16 [2, 4096, 64], replicated, may hold values from -0.09375 to 0.09375
- writing_intensity_map: bfloat16 [2, 4096, 64], replicated, may hold values from -0.09375 to 0.09375
- result_map: bfloat16 [2, 4096, 4096], P(None, 'tp', 'dp'), may hold values from -0.09375 to 0.09375
- fading_speed_exponent: float32 [2, 64], P(None, 'tp'), may hold values from 0 to 2.3
- fading_bias: float32 [2, 64], P(None, 'tp'), may hold values from -5 to -1
- entry_scaling: bfloat16 [2, 4096], P(None, 'dp'), may hold values from 0.099609375 to 1.8984375
- per_channel_scaling: bfloat16 [2, 64], replicated, may hold values from 0.099609375 to 1.8984375
- extra_shrink_exponent: float32 [2, 128, 4, 64], P(None, ('grp', 'dp'), None, 'tp'), parts along dimension 1, may hold values from -0.7 to 0
- memory_tensors: float32 [2, 128, 64, 4096], P(None, ('grp', 'dp'), None, 'tp'), parts along dimension 1, may hold values from -0.6 to 0.6
Outputs:
- mixed_tokens: bfloat16 [128, 4, 4096], P('grp', None, 'dp'), parts along dimension 0
- new_states: float32 [2, 128, 64, 4096], P(None, ('grp', 'dp'), None, 'tp'), parts along dimension 1
There are 2 independent parts, one for each index of `grp`. A program takes and returns all parts, laid end to end along the dimension named above; an argument that names none is the same for every part. Nothing has to cross between parts.
Inputs may be any that keep to these rules, and one draw needn't show every extreme that they name: `active_counts`: every sequence has at least one live slot, at least one sequence has 4.
All inputs are finite; a program needn't handle non-finite values. No bound on the sum of `active_counts` on one device may be relied on, other than what follows from the above.
Results may differ from a plain program's by a relative error of at most 0.018.
Values may be sent and summed in bfloat16 or wider, within the bound.
A program may use at most 128 MiB of HBM per device.

v0:
```python
import functools

import jax
import jax.numpy as jnp
from jax import lax
from jax.experimental import pallas as pl
from jax.experimental.pallas import tpu as pltpu
from jax.sharding import PartitionSpec as P

BLOCKS = 2
EPS = 1e-06
F32 = jnp.float32
BF16 = jnp.bfloat16
MESH = pl.DeviceIdType.MESH
VMEM = pl.BlockSpec(memory_space=pltpu.VMEM)


def greet(axis, peers):
    barrier = pltpu.get_barrier_semaphore()
    for peer in peers:
        pl.semaphore_signal(barrier, inc=1, device_id={axis: peer}, device_id_type=MESH)
    pl.semaphore_wait(barrier, len(peers))


def send(src, dst, send_sem, recv_sem, axis, peer):
    copy = pltpu.make_async_remote_copy(
        src_ref=src,
        dst_ref=dst,
        send_sem=send_sem,
        recv_sem=recv_sem,
        device_id={axis: peer},
        device_id_type=MESH,
    )
    copy.start()
    return copy


def params(cid):
    return pltpu.CompilerParams(
        collective_id=cid, has_side_effects=True, vmem_limit_bytes=48 * 1024 * 1024
    )


def gather_kernel(n, x_ref, o_ref, land, send_sem, recv_sem):
    me = lax.axis_index("dp")
    peers = [lax.rem(me + d, n) for d in range(1, n)]
    greet("dp", peers)
    copies = [
        send(x_ref, land.at[me], send_sem.at[d], recv_sem.at[d], "dp", peer)
        for d, peer in enumerate(peers)
    ]
    for copy in copies:
        copy.wait()
    o_ref[...] = land[...]
    o_ref[me] = x_ref[...]


def gather_counts(counts, n, cid):
    own = counts.shape[0]
    block = jnp.broadcast_to(jnp.pad(counts, (0, 128 - own))[None, :], (8, 128))
    out = pl.pallas_call(
        functools.partial(gather_kernel, n),
        out_shape=jax.ShapeDtypeStruct((n, 8, 128), jnp.int32),
        in_specs=[VMEM],
        out_specs=VMEM,
        scratch_shapes=[
            pltpu.VMEM((n, 8, 128), jnp.int32),
            pltpu.SemaphoreType.DMA((n - 1,)),
            pltpu.SemaphoreType.DMA((n - 1,)),
        ],
        compiler_params=params(cid),
        name="gather_counts",
    )(block)
    return out[:, 0, :own].reshape(n * own)


def dp_partners(n):
    me = lax.axis_index("dp")
    core = lax.rem(me, 2)
    partner = me + 1 - 2 * core
    return core, partner, [lax.rem(me + 2 * d, n) for d in range(1, n // 2)]


def reduce_over_dp(n, produce, x_refs, store, scratch, sems):
    chips = n // 2
    core, partner, others = dp_partners(n)
    send_sem, recv_sem = sems
    width = chips + 1
    rows = x_refs[0].shape[0] // 2
    mine = pl.multiple_of(core * rows, 16)
    theirs = pl.multiple_of((1 - core) * rows, 16)
    first, second, third = [], [], []

    def cross(a):
        x = x_refs[a]
        half, own, land, back = scratch[a]
        first[a].wait()
        for r in range(0, rows, 16):
            chunk = x[pl.ds(pl.multiple_of(mine + r, 16), 16), :].astype(F32) + half[pl.ds(r, 16), :].astype(F32)
            own[pl.ds(r, 16), :] = chunk.astype(BF16)
        second.append(
            [
                send(own, land.at[d], send_sem.at[a * width + 1 + d], recv_sem.at[a * width + 1 + d], "dp", peer)
                for d, peer in enumerate(others)
            ]
        )

    for a, x in enumerate(x_refs):
        produce(a)
        first.append(
            send(
                x.at[pl.ds(theirs, rows)], scratch[a][0], send_sem.at[a * width],
                recv_sem.at[a * width], "dp", partner,
            )
        )
        if a:
            cross(a - 1)
    cross(len(x_refs) - 1)
    for a in range(len(x_refs)):
        half, own, land, back = scratch[a]
        for copy in second[a]:
            copy.wait()
        for r in range(0, rows, 16):
            total = own[pl.ds(r, 16), :].astype(F32)
            for d in range(chips - 1):
                total = total + land[d, pl.ds(r, 16), :].astype(F32)
            own[pl.ds(r, 16), :] = total.astype(BF16)
        slot = a * width + chips
        third.append(send(own, back, send_sem.at[slot], recv_sem.at[slot], "dp", partner))
    for a in range(len(x_refs)):
        half, own, land, back = scratch[a]
        store(a, pl.ds(mine, rows), own[...])
        third[a].wait()
        store(a, pl.ds(theirs, rows), back[...])


def reduce_scratch(n, shapes):
    out = []
    for rows, cols in shapes:
        half = (rows // 2, cols)
        out += [
            pltpu.VMEM(half, BF16),
            pltpu.VMEM(half, BF16),
            pltpu.VMEM((n // 2 - 1,) + half, BF16),
            pltpu.VMEM(half, BF16),
        ]
    count = len(shapes) * (n // 2 + 1)
    return out + [pltpu.SemaphoreType.DMA((count,)), pltpu.SemaphoreType.DMA((count,))]


def proj_kernel(n, layer, h, gain, wab, wq, wk, wv, wz, main, small, wbuf, scaled, w_sem, *rest):
    feat, cols = wbuf.shape[1:]
    tile = min(256, cols)
    chunks = cols // tile
    loads = []
    for j in range(chunks):
        for i, w in enumerate((wq, wk, wv, wz)):
            at = pl.ds(j * tile, tile)
            load = pltpu.make_async_copy(w.at[layer, :, at], wbuf.at[i, :, at], w_sem.at[4 * j + i])
            load.start()
            loads.append(load)
    core, partner, others = dp_partners(n)
    greet("dp", [partner] + others)
    count = chunks + 1
    x_refs = rest[:count]
    scratch = [rest[count + 4 * a : count + 4 * a + 4] for a in range(count)]
    pair = wab.shape[2]

    def produce(a):
        x = x_refs[a]
        if a == 0:
            rows = h[...]
            bent = (rows * gain[...].astype(F32)).astype(BF16)
            scaled[...] = bent
            x[:, :pair] = jnp.dot(bent, wab[layer], preferred_element_type=F32).astype(BF16)
            squares = jnp.sum(rows * rows, axis=1, keepdims=True)
            x[:, pair:] = jnp.broadcast_to(squares, (rows.shape[0], x.shape[1] - pair)).astype(BF16)
            return
        j = a - 1
        for i in range(4):
            loads[4 * j + i].wait()
            x[:, i * tile : (i + 1) * tile] = jnp.dot(
                scaled[...], wbuf[i, :, j * tile : (j + 1) * tile], preferred_element_type=F32
            ).astype(BF16)

    def store(a, at, val):
        if a == 0:
            small[at, :] = val
        else:
            main[at, (a - 1) * 4 * tile : a * 4 * tile] = val

    reduce_over_dp(n, produce, x_refs, store, scratch, rest[-2:])


def project(h, gain, weights, wab, layer, n, cid):
    rows, feat = h.shape
    cols = weights[0].shape[2]
    tile = min(256, cols)
    chunks = cols // tile
    shapes = [(rows, wab.shape[2] + 128)] + [(rows, 4 * tile)] * chunks
    return pl.pallas_call(
        functools.partial(proj_kernel, n, layer),
        out_shape=[
            jax.ShapeDtypeStruct((rows, 4 * cols), BF16),
            jax.ShapeDtypeStruct(shapes[0], BF16),
        ],
        in_specs=[VMEM, VMEM, VMEM] + [pl.BlockSpec(memory_space=pl.ANY)] * 4,
        out_specs=[VMEM, VMEM],
        scratch_shapes=[
            pltpu.VMEM((4, feat, cols), BF16),
            pltpu.VMEM((rows, feat), BF16),
            pltpu.SemaphoreType.DMA((4 * chunks,)),
            *[pltpu.VMEM(shape, BF16) for shape in shapes],
            *reduce_scratch(n, shapes),
        ],
        compiler_params=params(cid),
        name="project",
    )(h, gain, wab, *weights)


def recur_kernel(
    width, size, head_size, heads_all, counts, where, main, small, pos_col, pos_row, speed, bias,
    shrink, gain, state, carried, y, new, q_s, k_s, v_s, z_s, dec_s, beta_s, o_s,
):
    group = state.shape[1]
    slots = q_s.shape[0] // (pl.num_programs(0) * group)
    tile = min(256, q_s.shape[1])
    cols = q_s.shape[1]
    row = lax.broadcasted_iota(jnp.int32, (tile, tile), 0) // head_size
    col = lax.broadcasted_iota(jnp.int32, (tile, tile), 1) // head_size
    blocks = (row == col).astype(BF16)

    @pl.when(pl.program_id(0) == 0)
    def _():
        own = q_s.shape[0]
        packed = main.shape[0]
        pick = (pos_col[...] == lax.broadcasted_iota(jnp.int32, (own, packed), 1)).astype(BF16)
        few = jnp.dot(pick, small[...], preferred_element_type=F32)
        factor = lax.rsqrt(few[:, 2 * heads_all : 2 * heads_all + 1] / width + EPS)
        heads = speed.shape[1]
        first = where[1] * heads
        ones = lax.broadcasted_iota(jnp.int32, (heads_all, cols), 0)
        lane = lax.broadcasted_iota(jnp.int32, (heads_all, cols), 1) // head_size
        spread_all = (ones == lane + first).astype(BF16)
        spread = (
            lax.broadcasted_iota(jnp.int32, (heads, cols), 0)
            == lax.broadcasted_iota(jnp.int32, (heads, cols), 1) // head_size
        ).astype(F32)
        pa = jnp.dot(few[:, :heads_all].astype(BF16), spread_all, preferred_element_type=F32) * factor
        pb = jnp.dot(
            few[:, heads_all : 2 * heads_all].astype(BF16), spread_all, preferred_element_type=F32
        ) * factor
        exact = functools.partial(
            jnp.dot, precision=lax.Precision.HIGHEST, preferred_element_type=F32
        )
        rate = exact(jnp.broadcast_to(jnp.exp(speed[...]), (8, heads)), spread)[:1]
        offset = exact(jnp.broadcast_to(bias[...], (8, heads)), spread)[:1]
        extra = exact(shrink[...], spread)
        arg = pa + offset
        soft = jnp.maximum(arg, 0.0) + jnp.log1p(jnp.exp(-jnp.abs(arg)))
        dec_s[...] = jnp.exp(extra - rate * soft)
        beta_s[...] = jax.nn.sigmoid(pb)
        for j in range(cols // tile):
            here = slice(j * tile, (j + 1) * tile)
            chunk = jnp.dot(
                pick, main[:, j * 4 * tile : (j + 1) * 4 * tile], preferred_element_type=F32
            ) * factor
            for i, dst in enumerate((q_s, k_s, v_s, z_s)):
                val = chunk[:, i * tile : (i + 1) * tile]
                val = val * jax.nn.sigmoid(val)
                if i < 2:
                    total = jnp.dot((val * val).astype(BF16), blocks, preferred_element_type=F32)
                    val = val * lax.rsqrt(total + EPS)
                    if i == 0:
                        val = val * head_size ** (-0.5)
                dst[:, here] = val
        o_s[...] = jnp.zeros_like(o_s)

    new[...] = state[...]
    key_row = lax.broadcasted_iota(jnp.int32, (size, tile), 0)
    key_col = lax.rem(lax.broadcasted_iota(jnp.int32, (size, tile), 1), head_size)
    diag = key_row == key_col
    for g in range(group):
        seq = pl.program_id(0) * group + g
        for t in range(slots):

            @pl.when(t < counts[seq])
            def _():
                at = pl.ds(seq * slots + t, 1)
                for j in range(cols // tile):
                    here = slice(j * tile, (j + 1) * tile)
                    kq = jnp.concatenate(
                        [
                            jnp.where(diag, jnp.broadcast_to(k_s[at, here], (size, tile)), 0.0),
                            jnp.where(diag, jnp.broadcast_to(q_s[at, here], (size, tile)), 0.0),
                        ],
                        axis=0,
                    ).astype(BF16)
                    kq = jnp.dot(kq, blocks, preferred_element_type=F32)
                    kmat, qmat = kq[:size], kq[size:]
                    decayed = new[0, g, :, here] * dec_s[at, here]
                    guess = jnp.sum(decayed * kmat, axis=0, keepdims=True)
                    fresh = beta_s[at, here] * (v_s[at, here] - guess)
                    updated = decayed + kmat * fresh
                    new[0, g, :, here] = updated
                    o_s[at, here] = jnp.sum(updated * qmat, axis=0, keepdims=True)

    @pl.when(pl.program_id(0) == pl.num_programs(0) - 1)
    def _():
        own = q_s.shape[0]
        packed = main.shape[0]
        place = (lax.broadcasted_iota(jnp.int32, (packed, own), 0) == pos_row[...]).astype(BF16)
        for j in range(cols // tile):
            here = slice(j * tile, (j + 1) * tile)
            val = o_s[:, here]
            total = jnp.dot((val * val).astype(BF16), blocks, preferred_element_type=F32)
            val = val * lax.rsqrt(total / head_size + EPS) * gain[:, here] * z_s[:, here]
            y[:, here] = jnp.dot(place, val.astype(BF16), preferred_element_type=F32).astype(BF16)


def recur(counts, where, main, small, pos, speed, bias, shrink, gain, states, carried, layer, width, heads_all):
    own_seqs = counts.shape[0]
    group = 2 if own_seqs % 2 == 0 else 1
    packed = main.shape[0]
    size, cols = states.shape[2:]
    own = pos.shape[0]
    heads = speed.shape[1]
    whole = lambda shape: pl.BlockSpec(shape, lambda s, *_: (0,) * len(shape))
    here = pl.BlockSpec((1, group, size, cols), lambda s, *_: (layer, s, 0, 0))
    args = [main, small, pos[:, None], pos[None, :], speed, bias, shrink, gain]
    specs = [whole(a.shape) for a in args] + [here]
    kernel = functools.partial(recur_kernel, width, size, cols // heads, heads_all)
    if carried is None:
        body = lambda *refs: kernel(*refs[:11], None, *refs[11:])
        more, alias = [], {}
    else:
        body = kernel
        more, alias = [carried], {11: 1}
        specs = specs + [pl.BlockSpec(memory_space=pl.ANY)]
    return pl.pallas_call(
        body,
        out_shape=[
            jax.ShapeDtypeStruct((packed, cols), BF16),
            jax.ShapeDtypeStruct(states.shape, F32),
        ],
        grid_spec=pltpu.PrefetchScalarGridSpec(
            num_scalar_prefetch=2,
            grid=(own_seqs // group,),
            in_specs=specs,
            out_specs=[whole((packed, cols)), here],
            scratch_shapes=[pltpu.VMEM((own, cols), F32) for _ in range(7)],
        ),
        input_output_aliases=alias,
        name="recur",
    )(counts, where, *args, states, *more)


def mix_kernel(
    n, m, layer, y, w, h, out, wbuf, w_sem, gated, part, land, own, gath,
    send_a, recv_a, send_b, recv_b, *rest,
):
    load = pltpu.make_async_copy(w.at[layer], wbuf, w_sem)
    load.start()
    me = lax.axis_index("tp")
    peers = [lax.rem(me + d, m) for d in range(1, m)]
    core, partner, others = dp_partners(n)
    barrier = pltpu.get_barrier_semaphore()
    for axis, group in (("dp", [partner] + others), ("tp", peers)):
        for peer in group:
            pl.semaphore_signal(barrier, inc=1, device_id={axis: peer}, device_id_type=MESH)
    pl.semaphore_wait(barrier, 1 + len(others) + len(peers))

    def store(a, at, val):
        gated[at, :] = val

    reduce_over_dp(n, lambda a: None, [y], store, [rest[0:4]], rest[4:6])
    load.wait()
    rows = part.shape[1]
    mixed = jnp.dot(gated[...], wbuf[...], preferred_element_type=F32)
    for j in range(m):
        part[j] = mixed[j * rows : (j + 1) * rows].astype(BF16)
    copies = [
        send(part.at[peer], land.at[d], send_a.at[d], recv_a.at[d], "tp", peer)
        for d, peer in enumerate(peers)
    ]
    total = part[me].astype(F32)
    for d, copy in enumerate(copies):
        copy.wait()
        total = total + land[d].astype(F32)
    own[...] = total.astype(BF16)
    copies = [
        send(own, gath.at[me], send_b.at[d], recv_b.at[d], "tp", peer)
        for d, peer in enumerate(peers)
    ]
    for copy in copies:
        copy.wait()
    gath[me] = own[...]
    for j in range(m):
        at = slice(j * rows, (j + 1) * rows)
        out[at, :] = (h[at, :] + gath[j].astype(F32)).astype(BF16).astype(F32)


def mix(y, w, h, layer, n, m, cid):
    packed, feat = h.shape
    rows = packed // m
    return pl.pallas_call(
        functools.partial(mix_kernel, n, m, layer),
        out_shape=jax.ShapeDtypeStruct(h.shape, F32),
        in_specs=[VMEM, pl.BlockSpec(memory_space=pl.ANY), VMEM],
        out_specs=VMEM,
        scratch_shapes=[
            pltpu.VMEM(w.shape[1:], BF16),
            pltpu.SemaphoreType.DMA,
            pltpu.VMEM(y.shape, BF16),
            pltpu.VMEM((m, rows, feat), BF16),
            pltpu.VMEM((m - 1, rows, feat), BF16),
            pltpu.VMEM((rows, feat), BF16),
            pltpu.VMEM((m, rows, feat), BF16),
            *[pltpu.SemaphoreType.DMA((m - 1,)) for _ in range(4)],
            *reduce_scratch(n, [y.shape]),
        ],
        compiler_params=params(cid),
        name="mix",
    )(y, w, h)


def body(
    n,
    m,
    resid,
    counts,
    wq,
    wk,
    wv,
    wz,
    wa,
    wb,
    wo,
    speed,
    bias,
    scaling,
    channel,
    shrink,
    states,
):
    all_seqs, slots, feat = resid.shape
    own_seqs = counts.shape[0]
    own = own_seqs * slots
    heads = speed.shape[1]
    live_rows = all_seqs * 3 // 2
    step = -(-live_rows // m)
    step = -(-step // 8) * 8
    while step * m % 32:
        step += 8
    packed = step * m
    dp = lax.axis_index("dp")
    where = jnp.stack([dp, lax.axis_index("tp")]).astype(jnp.int32)
    every = gather_counts(counts, n, 1)
    cut = lambda w: lax.dynamic_slice_in_dim(w, dp * feat, feat, 1)
    wab = jnp.concatenate([cut(wa), cut(wb)], axis=2)
    before = lax.broadcasted_iota(jnp.int32, (all_seqs, all_seqs), 1) < lax.broadcasted_iota(
        jnp.int32, (all_seqs, all_seqs), 0
    )
    start = jnp.sum(jnp.where(before, every[None, :], 0), axis=1)
    slot = lax.broadcasted_iota(jnp.int32, (all_seqs, slots), 1)
    pos = jnp.where(slot < every[:, None], start[:, None] + slot, -1).reshape(all_seqs * slots)
    pos_own = lax.dynamic_slice_in_dim(pos, dp * own, own, 0)
    onehot = (lax.broadcasted_iota(jnp.int32, (packed, all_seqs * slots), 0) == pos[None, :]).astype(BF16)
    flat = resid.reshape(all_seqs * slots, feat)
    h = jnp.dot(onehot, flat, preferred_element_type=F32)
    carried = None
    for l in range(BLOCKS):
        main, small = project(h, scaling[l][None], (wq, wk, wv, wz), wab, l, n, 2 + 2 * l)
        gain = jnp.tile(channel[l].astype(F32), heads)[None]
        y, carried = recur(
            counts, where, main, small, pos_own, speed[l][None], bias[l][None],
            shrink[l].reshape(own, heads), gain, states, carried, l, feat * n, wa.shape[2],
        )
        h = mix(y, wo, h, l, n, m, 3 + 2 * l)
    back = lax.dot_general(
        onehot, h.astype(BF16), (((0,), (0,)), ((), ())), preferred_element_type=F32
    )
    out = jnp.where(pos[:, None] >= 0, back, flat.astype(F32)).astype(BF16)
    return out.reshape(all_seqs, slots, feat), carried


def solution(mesh):
    in_specs = (
        P("grp", None, "dp"),
        P(("grp", "dp")),
        P(None, "dp", "tp"),
        P(None, "dp", "tp"),
        P(None, "dp", "tp"),
        P(None, "dp", "tp"),
        P(),
        P(),
        P(None, "tp", "dp"),
        P(None, "tp"),
        P(None, "tp"),
        P(None, "dp"),
        P(),
        P(None, ("grp", "dp"), None, "tp"),
        P(None, ("grp", "dp"), None, "tp"),
    )
    out_specs = (P("grp", None, "dp"), P(None, ("grp", "dp"), None, "tp"))
    run = functools.partial(body, mesh.shape["dp"], mesh.shape["tp"])
    return jax.shard_map(run, mesh=mesh, in_specs=in_specs, out_specs=out_specs, check_vma=False)
```

profile of v0, /device:TPU:0, one launch (start us, length us, event | category | flops | bytes accessed | tf_op | source)
XLA Modules:
  0.0 127.9 jit_solution(3065554608145373025)
XLA Ops:
  0.7 1.1 constant_dynamic-slice_fusion
  1.8 0.3 copy.30
  2.1 0.3 copy.31
  2.4 0.3 pad_maximum_fusion.wab
  2.7 4.7 %gather_counts.1 = s32[4,8,128]{2,1,0:T(8,128)S(1)} custom-call(s32[8,128]{1,0:T(8,128)S(1)} %broadcast_in_dim.39.x_ref), custom_call_target="tpu_custom_call" | custom-call | tf_op jit(solution)/shard_map/gather_counts/pallas_call | solution.py:61
  7.5 0.1 select_reduce_fusion
  7.8 0.1 reshape.76
  7.9 0.2 fusion.2.h
  8.2 2.2 %copy-done = bf16[2,1024,1024]{2,1,0:T(8,128)(2,1)S(1)} copy-done((bf16[2,1024,1024]{2,1,0:T(8,128)(2,1)S(1)}, bf16[2,1024,1024]{2,1,0:T(8,128)(2,1)}, u32[]{:S(2)}) %copy-start) | copy-done | bytes 4194328
  10.4 16.0 %project.2 = (bf16[96,4096]{1,0:T(8,128)(2,1)S(1)}, bf16[96,256]{1,0:T(8,128)(2,1)S(1)}) custom-call(f32[96,1024]{1,0:T(8,128)S(1)} %fusion.2.h, bf16[1,1024]{1,0:T(2,128)(2,1)S(1)} %get-tuple-element.21.gain, bf16[2,1024,128]{2,1,0:T(8,128)(2,1)S(1)} %pad_maximum_fusion.wab, bf16[2,1024,1024]{2,1,0:T(8,128)(2,1)S(1)} %copy-done, bf16[2,1024,1024]{2,1,0:T(8,128)(2,1)} %wk.3, ...), custom_call_target="tpu_custom_call" | custom-call | tf_op jit(solution)/shard_map/project/pallas_call | solution.py:201
  26.4 0.9 copy-done.4
  27.3 0.6 copy-done.8
  27.9 0.6 dynamic-slice_bitcast_fusion
  28.5 0.7 copy.28.refs_4_.pos_col
  29.2 0.6 pad_add_fusion.refs_1_.where
  29.8 0.6 fusion.7
  30.4 0.6 fusion.5
  31.0 0.7 broadcast_in_dim_tile.6.refs_9_
  31.7 14.0 %recur.2 = (bf16[96,1024]{1,0:T(8,128)(2,1)}, f32[2,16,64,1024]{3,2,1,0:T(8,128)}) custom-call(s32[16]{0:T(128)} %counts.1, s32[2]{0:T(128)} %pad_add_fusion.refs_1_.where, bf16[96,4096]{1,0:T(8,128)(2,1)} %copy-done.4, bf16[96,256]{1,0:T(8,128)(2,1)} %copy-done.8, s32[64,1]{1,0:T(8,128)} %copy.28.refs_4_.pos_col, ...), custom_call_target="tpu_custom_call" | custom-call | tf_op jit(solution)/shard_map/recur/pallas_call | solution.py:340
  45.7 2.3 %copy-done.2 = bf16[2,1024,1024]{2,1,0:T(8,128)(2,1)S(1)} copy-done((bf16[2,1024,1024]{2,1,0:T(8,128)(2,1)S(1)}, bf16[2,1024,1024]{2,1,0:T(8,128)(2,1)}, u32[]{:S(2)}) %copy-start.2) | copy-done | bytes 4194328
  48.1 1.1 copy-done.7
  49.2 21.6 %mix.2.h = f32[96,1024]{1,0:T(8,128)S(1)} custom-call(bf16[96,1024]{1,0:T(8,128)(2,1)S(1)} %copy-done.7, bf16[2,1024,1024]{2,1,0:T(8,128)(2,1)S(1)} %copy-done.2, f32[96,1024]{1,0:T(8,128)S(1)} %fusion.2.h), custom_call_target="tpu_custom_call" | custom-call | tf_op jit(solution)/shard_map/mix/pallas_call | solution.py:406
  70.8 15.7 %project.3 = (bf16[96,4096]{1,0:T(8,128)(2,1)S(1)}, bf16[96,256]{1,0:T(8,128)(2,1)S(1)}) custom-call(f32[96,1024]{1,0:T(8,128)S(1)} %mix.2.h, bf16[1,1024]{1,0:T(2,128)(2,1)S(1)} %get-tuple-element.20.gain, bf16[2,1024,128]{2,1,0:T(8,128)(2,1)S(1)} %pad_maximum_fusion.wab, bf16[2,1024,1024]{2,1,0:T(8,128)(2,1)S(1)} %copy-done.1, bf16[2,1024,1024]{2,1,0:T(8,128)(2,1)} %wk.3, ...), custom_call_target="tpu_custom_call" | custom-call | tf_op jit(solution)/shard_map/project/pallas_call | solution.py:201
  86.5 0.9 copy-done.5
  87.4 0.6 copy-done.9
  88.0 0.7 broadcast_in_dim_tile.7.gain
  88.7 14.2 %recur.3 = (bf16[96,1024]{1,0:T(8,128)(2,1)}, f32[2,16,64,1024]{3,2,1,0:T(8,128)}) custom-call(s32[16]{0:T(128)} %counts.1, s32[2]{0:T(128)} %pad_add_fusion.refs_1_.where, bf16[96,4096]{1,0:T(8,128)(2,1)} %copy-done.5, bf16[96,256]{1,0:T(8,128)(2,1)} %copy-done.9, s32[64,1]{1,0:T(8,128)} %copy.28.refs_4_.pos_col, ...), custom_call_target="tpu_custom_call", output_to_operand_aliasing={{1}: (11, {})} | custom-call | tf_op jit(solution)/shard_map/recur/pallas_call | solution.py:340
  102.9 2.2 %copy-done.3 = bf16[2,1024,1024]{2,1,0:T(8,128)(2,1)S(1)} copy-done((bf16[2,1024,1024]{2,1,0:T(8,128)(2,1)S(1)}, bf16[2,1024,1024]{2,1,0:T(8,128)(2,1)}, u32[]{:S(2)}) %copy-start.3) | copy-done | bytes 4194328
  105.0 0.9 copy-done.6
  106.0 20.6 %mix.3 = f32[96,1024]{1,0:T(8,128)S(1)} custom-call(bf16[96,1024]{1,0:T(8,128)(2,1)S(1)} %copy-done.6, bf16[2,1024,1024]{2,1,0:T(8,128)(2,1)S(1)} %copy-done.3, f32[96,1024]{1,0:T(8,128)S(1)} %mix.2.h), custom_call_target="tpu_custom_call" | custom-call | tf_op jit(solution)/shard_map/mix/pallas_call | solution.py:406
  126.6 0.3 fusion
  126.9 1.0 reshape.77
  (36 shorter events, 0.4 us)
Async XLA Ops:
  0.6 2.0 %copy-start.13 = (s32[16]{0:T(128)S(1)}, s32[16]{0:T(128)}, u32[]{:S(2)}) copy-start(s32[16]{0:T(128)} %counts.1) | copy-start | bytes 196
  0.6 7.2 %copy-start.10 = (bf16[64,4,1024]{2,1,0:T(4,128)(2,1)S(1)}, bf16[64,4,1024]{2,1,0:T(4,128)(2,1)}, u32[]{:S(2)}) copy-start(bf16[64,4,1024]{2,1,0:T(4,128)(2,1)} %param.15) | copy-start | bytes 1572868
  0.7 7.5 %copy-start.12 = (bf16[2,1024]{1,0:T(2,128)(2,1)S(1)}, bf16[2,1024]{1,0:T(2,128)(2,1)}, u32[]{:S(2)}) copy-start(bf16[2,1024]{1,0:T(2,128)(2,1)} %param.26) | copy-start | bytes 12292
  8.2 2.2 %copy-start = (bf16[2,1024,1024]{2,1,0:T(8,128)(2,1)S(1)}, bf16[2,1024,1024]{2,1,0:T(8,128)(2,1)}, u32[]{:S(2)}) copy-start(bf16[2,1024,1024]{2,1,0:T(8,128)(2,1)} %wq.3) | copy-start | bytes 12582916
  10.4 19.4 %copy-start.15 = (f32[2,16]{1,0:T(2,128)S(1)}, f32[2,16]{1,0:T(2,128)}, u32[]{:S(2)}) copy-start(f32[2,16]{1,0:T(2,128)} %param.25) | copy-start | bytes 388
  10.4 19.4 %copy-start.16 = (f32[2,16]{1,0:T(2,128)S(1)}, f32[2,16]{1,0:T(2,128)}, u32[]{:S(2)}) copy-start(f32[2,16]{1,0:T(2,128)} %param.24) | copy-start | bytes 388
  10.4 20.0 %copy-start.11 = (f32[2,16,4,16]{3,2,1,0:T(4,128)S(1)}, f32[2,16,4,16]{3,2,1,0:T(4,128)}, u32[]{:S(2)}) copy-start(f32[2,16,4,16]{3,2,1,0:T(4,128)} %param.28) | copy-start | bytes 24580
  10.4 20.7 %copy-start.14 = (bf16[2,64]{1,0:T(2,128)(2,1)S(1)}, bf16[2,64]{1,0:T(2,128)(2,1)}, u32[]{:S(2)}) copy-start(bf16[2,64]{1,0:T(2,128)(2,1)} %param.27) | copy-start | bytes 772
  26.4 0.9 copy-start.4
  27.3 0.6 copy-start.8
  45.7 25.1 %copy-start.1 = (bf16[2,1024,1024]{2,1,0:T(8,128)(2,1)S(1)}, bf16[2,1024,1024]{2,1,0:T(8,128)(2,1)}, u32[]{:S(2)}) copy-start(bf16[2,1024,1024]{2,1,0:T(8,128)(2,1)} %wq.3) | copy-start | bytes 12582916
  45.7 2.3 %copy-start.2 = (bf16[2,1024,1024]{2,1,0:T(8,128)(2,1)S(1)}, bf16[2,1024,1024]{2,1,0:T(8,128)(2,1)}, u32[]{:S(2)}) copy-start(bf16[2,1024,1024]{2,1,0:T(8,128)(2,1)} %w.3) | copy-start | bytes 12582916
  48.1 1.1 copy-start.7
  86.5 0.9 copy-start.5
  87.4 0.6 copy-start.9
  102.9 2.2 %copy-start.3 = (bf16[2,1024,1024]{2,1,0:T(8,128)(2,1)S(1)}, bf16[2,1024,1024]{2,1,0:T(8,128)(2,1)}, u32[]{:S(2)}) copy-start(bf16[2,1024,1024]{2,1,0:T(8,128)(2,1)} %w.3) | copy-start | bytes 12582916
  105.0 0.9 copy-start.6
where the time goes:
time: 129 us; the launch traced here: 128 us
  Pallas kernels  107 us (83%)
  local copies, waits for them, and re-layouts  18.6 us (14%)
    pallas_call x2, Pallas kernels, mix(): pl.pallas_call(functools.partial(mix_kernel, n, m, layer), out_shape=jax....  42.2 us
    pallas_call x2, Pallas kernels, project(): pl.pallas_call(functools.partial(proj_kernel, n, layer), out_shape=[jax.S...  31.7 us
    pallas_call x2, Pallas kernels, recur(): pl.pallas_call(body, out_shape=[jax.ShapeDtypeStruct((packed, cols), BF16...  28.2 us
    unnamed x36, local copies, waits for them, and re-layouts  12.3 us
    pallas_call x1, Pallas kernels, gather_counts(): pl.pallas_call(functools.partial(gather_kernel, n), out_shape=jax.ShapeDt...  4.68 us

commit v1 on v0

v1 whole, which is shorter than its diff:
```python
import functools
import types

import jax
import jax.numpy as jnp
from jax import lax
from jax.experimental import pallas as pl
from jax.experimental.pallas import tpu as pltpu
from jax.sharding import PartitionSpec as P

BLOCKS = 2
EPS = 1e-06
F32 = jnp.float32
BF16 = jnp.bfloat16
MESH = pl.DeviceIdType.MESH
VMEM = pl.BlockSpec(memory_space=pltpu.VMEM)
HBM = pl.BlockSpec(memory_space=pltpu.HBM)
SMEM = pl.BlockSpec(memory_space=pltpu.SMEM)


def iota(shape, dim):
    return lax.broadcasted_iota(jnp.int32, shape, dim)


def dot(a, b):
    return jnp.dot(a, b, preferred_element_type=F32)


def exact(a, b):
    return jnp.dot(a, b, precision=lax.Precision.HIGHEST, preferred_element_type=F32)


def tiles(ref, count):
    return jnp.concatenate([ref] * count, axis=0)


def sizes(n, m, resid, counts, wq, speed):
    c = types.SimpleNamespace(n=n, m=m)
    c.seqs, c.slots, c.feat = resid.shape
    c.own_seqs = counts.shape[0]
    c.cols = wq.shape[2]
    c.heads = speed.shape[1]
    c.size = c.cols // c.heads
    c.own = c.own_seqs * c.slots
    c.rows = c.seqs * c.slots
    c.packed = c.seqs * 3 // 2
    c.chips = n // 2
    c.per_chip = 2 * c.own_seqs
    c.chip_win = c.packed - (c.chips - 1) * c.per_chip
    c.win = c.packed - (n - 1) * c.own_seqs
    c.tile = min(256, c.cols)
    c.chunks = c.cols // c.tile
    c.per_tile = c.tile // c.size
    c.groups = c.own_seqs // c.per_tile
    c.parts = 4
    c.part = c.feat // c.parts
    c.lanes = -(-c.seqs // 128) * 128
    return c


def main_kernel(
    c, counts, flat, wq, wk, wv, wz, wa, wb, wo, speed, bias, scaling, channel, shrink, states,
    kx, wx, gx, hx, hot, *scratch,
):
    s = types.SimpleNamespace(**dict(zip(c.names, scratch)))
    n, m, chips, tile = c.n, c.m, c.chips, c.tile
    me = lax.axis_index("dp")
    z = lax.axis_index("tp")
    core = lax.rem(me, 2)
    chip = lax.div(me, 2)
    partner = me + 1 - 2 * core
    others = [lax.rem(me + 2 * d, n) for d in range(1, chips)]
    sources = [lax.rem(me + n - 2 * d, n) for d in range(1, chips)]
    half = m // 2
    left = z < half
    depth = jnp.where(left, z, m - 1 - z)
    toward = jnp.where(left, z + 1, z - 1)
    away = lax.rem(jnp.where(left, z - 1, z + 1) + m, m)
    centre = depth == half - 1

    def remote(src, dst, send_sem, recv_sem, axis, peer):
        return pltpu.make_async_remote_copy(
            src_ref=src, dst_ref=dst, send_sem=send_sem, recv_sem=recv_sem,
            device_id={axis: peer}, device_id_type=MESH,
        )

    def load(src, dst, sem):
        copy = pltpu.make_async_copy(src, dst, sem)
        copy.start()
        return copy

    feats = pl.ds(pl.multiple_of(me * c.feat, 16), c.feat)
    early = [
        load(src, dst, s.small_sem.at[i])
        for i, (src, dst) in enumerate(
            [
                (flat, s.flat), (scaling, s.scaling), (wa.at[:, feats, :], s.wa), (wb.at[:, feats, :], s.wb),
                (speed, s.speed), (bias, s.bias), (channel, s.channel), (shrink, s.shrink),
            ]
        )
    ]
    w_loads, wo_loads, state_loads = {}, {}, {}

    def load_weights(l):
        for j in range(c.chunks):
            for i, w in enumerate((wq, wk, wv, wz)):
                at = pl.ds(j * tile, tile)
                w_loads[l, j, i] = load(w.at[l, :, at], s.w.at[l, i, :, at], s.w_sem.at[l, j, i])

    def load_rest(l):
        state_loads[l] = load(states.at[l], s.states.at[l], s.state_sem.at[l])
        wo_loads[l] = load(wo.at[l], s.wo.at[l], s.wo_sem.at[l])

    load_weights(0)

    barrier = pltpu.get_barrier_semaphore()
    dp_peers = [lax.rem(me + d, n) for d in range(1, n)]
    for axis, peers in (("dp", dp_peers), ("tp", [lax.rem(z + 1, m), lax.rem(z + m - 1, m)])):
        for peer in peers:
            pl.semaphore_signal(barrier, inc=1, device_id={axis: peer}, device_id_type=MESH)
    pl.semaphore_wait(barrier, n + 1)

    lane = iota((8, c.lanes), 1) - me * c.own_seqs
    mine = jnp.zeros((8, c.lanes), jnp.int32)
    for i in range(c.own_seqs):
        mine = jnp.where(lane == i, counts[i], mine)
    s.counts[me] = mine
    swaps = [
        remote(s.counts.at[me], s.counts.at[me], s.count_s.at[d], s.count_r.at[d], "dp", peer)
        for d, peer in enumerate(dp_peers)
    ]
    for copy in swaps:
        copy.start()

    row = lax.div(iota((tile, tile), 0), c.size)
    col = lax.div(iota((tile, tile), 1), c.size)
    s.blocks[...] = (row == col).astype(BF16)
    for h in range(c.per_tile):
        s.spread[h] = (
            iota((tile, tile), 0) == h * c.size + lax.rem(iota((tile, tile), 1), c.size)
        ).astype(BF16)
    for g in range(c.groups):
        r = lax.rem(iota((2 * c.own, tile), 0), c.own_seqs)
        k = g * c.per_tile + lax.div(iota((2 * c.own, tile), 1), c.size)
        s.mask[g] = (r == k).astype(BF16)
    load_rest(0)
    for copy in early:
        copy.wait()
    all_heads = wa.shape[2]
    ab = 2 * all_heads
    for l in range(BLOCKS):
        at_a = (iota((all_heads, ab), 0) == iota((all_heads, ab), 1)).astype(BF16)
        at_b = (iota((all_heads, ab), 0) + all_heads == iota((all_heads, ab), 1)).astype(BF16)
        s.wab[l] = (dot(s.wa[l], at_a) + dot(s.wb[l], at_b)).astype(BF16)

    for copy in swaps:
        copy.wait()
    total = s.counts[0]
    for d in range(1, n):
        total = total + s.counts[d]
    row_counts = total.astype(F32)
    row_bf16 = row_counts.astype(BF16)

    def columns(count, seq, slot):
        lanes = iota((count, c.lanes), 1)
        all_counts = jnp.broadcast_to(row_counts[:1], (count, c.lanes))
        start = jnp.sum(jnp.where(lanes < seq, all_counts, 0.0), axis=1, keepdims=True)
        size = jnp.sum(jnp.where(lanes == seq, all_counts, 0.0), axis=1, keepdims=True)
        slot = slot[:, :1].astype(F32)
        return start + slot, slot < size

    def rows_of(seq, slot):
        index = iota(seq.shape, 0)
        start = dot(row_bf16, (index < seq).astype(BF16))[:1]
        size = dot(row_bf16, (index == seq).astype(BF16))[:1]
        slot = slot[:1].astype(F32)
        return start + slot, slot < size

    shape = (c.lanes, c.rows)
    pos, live = rows_of(lax.div(iota(shape, 1), c.slots), lax.rem(iota(shape, 1), c.slots))
    into = jnp.where((iota((c.packed, c.rows), 0).astype(F32) == pos) & live, 1.0, 0.0).astype(BF16)
    h0 = dot(into, s.flat[...])
    s.h[...] = h0
    s.scaled[0] = (h0 * s.scaling[...].astype(F32)[:1]).astype(BF16)

    def produce(l, j, acc):
        for i in range(4):
            if acc is None:
                w_loads[l, j, i].wait()
                val = dot(s.scaled[l], s.w[l, i, :, j * tile : (j + 1) * tile])
            else:
                val = acc(j, i)
            s.x[l, j, i // 2, :, (i % 2) * tile : (i % 2 + 1) * tile] = val.astype(BF16)
        first(l, j).start()

    def produce_small(l):
        h = s.h[...]
        s.x_small[l, 0] = dot(s.scaled[l], s.wab[l]).astype(BF16)
        squares = jnp.sum(h * h, axis=1, keepdims=True)
        s.x_small[l, 1] = jnp.broadcast_to(squares, (c.packed, ab)).astype(BF16)
        first(l, -1).start()

    def bufs(l, j):
        if j < 0:
            return s.x_small.at[l], s.pair_small.at[l], s.sum_small.at[l], s.far_small.at[l], s.out_small.at[l], s.fin_small.at[l]
        return s.x.at[l, j], s.pair.at[l, j], s.sum.at[l, j], s.far.at[l, j], s.out.at[l, j], s.fin.at[l, j]

    def first(l, j):
        x, pair, *_ = bufs(l, j)
        return remote(x.at[1 - core], pair, s.first_s.at[l, j + 1], s.first_r.at[l, j + 1], "dp", partner)

    def second(l, j, d):
        _, _, own, far, *_ = bufs(l, j)
        there = pl.multiple_of(lax.div(others[d], 2) * c.per_chip, 16)
        return remote(
            own.at[pl.ds(there, c.chip_win)], far.at[d], s.second_s.at[l, j + 1, d], s.second_r.at[l, j + 1, d],
            "dp", others[d],
        )

    def third(l, j):
        *_, out, fin = bufs(l, j)
        return remote(out, fin.at[core], s.third_s.at[l, j + 1], s.third_r.at[l, j + 1], "dp", partner)

    def cross(l, j):
        x, pair, own, *_ = bufs(l, j)
        first(l, j).wait()
        own[...] = (x[core].astype(F32) + pair[...].astype(F32)).astype(BF16)
        for d in range(chips - 1):
            second(l, j, d).start()

    def finish(l, j):
        x, pair, own, far, out, fin = bufs(l, j)
        for d in range(chips - 1):
            second(l, j, d).wait()

        def reduced(which):
            at = pl.multiple_of(which * c.own_seqs, 16)
            val = own[pl.ds(pl.multiple_of(chip * c.per_chip + at, 16), c.win), :].astype(F32)
            for d in range(chips - 1):
                val = val + far[d, pl.ds(at, c.win), :].astype(F32)
            return val.astype(BF16)

        out[...] = reduced(1 - core)
        third(l, j).start()
        fin[core] = reduced(core)

    def prepare(l):
        third(l, -1).wait()
        pick = s.pick[...]
        heads = c.heads
        few = dot(pick, s.fin_small[l, 0]).astype(BF16)
        squares = dot(pick, s.fin_small[l, 1])[:, :1]
        factor = lax.rsqrt(squares / (c.feat * n) + EPS)
        s.factor[...] = jnp.broadcast_to(factor, s.factor.shape)
        at = iota((ab, heads), 1) + z * heads
        pa = dot(few, (iota((ab, heads), 0) == at).astype(BF16)) * factor
        pb = dot(few, (iota((ab, heads), 0) == at + all_heads).astype(BF16)) * factor
        arg = pa + s.bias[...][l : l + 1]
        soft = jnp.maximum(arg, 0.0) + jnp.log1p(jnp.exp(-jnp.abs(arg)))
        extra = jnp.concatenate([s.shrink[l, :, t, :] for t in range(c.slots)], axis=0)
        dec = jnp.exp(extra - jnp.exp(s.speed[...][l : l + 1]) * soft)
        dec = jnp.where(s.live[:, :1] > 0.0, dec, 1.0)
        wide = (iota((heads, c.cols), 0) == lax.div(iota((heads, c.cols), 1), c.size)).astype(F32)
        s.dec[...] = exact(dec, wide)
        s.beta[...] = exact(jax.nn.sigmoid(pb), wide)

    def recur(l, j):
        at = slice(j * tile, (j + 1) * tile)
        third(l, j).wait()
        pick = s.pick[...]
        factor = s.factor[:, :1]
        kept = []
        for i in range(4):
            val = dot(pick, s.fin[l, j, i // 2, :, (i % 2) * tile : (i % 2 + 1) * tile]) * factor
            val = val * jax.nn.sigmoid(val)
            if i < 2:
                total = dot((val * val).astype(BF16), s.blocks[...])
                val = val * lax.rsqrt(total + EPS)
                if i == 0:
                    val = val * c.size ** (-0.5)
            kept.append(val)
        q, k, v, zed = kept
        both = jnp.concatenate([k, q], axis=0).astype(BF16)
        kx[l, :, at] = both[: c.own]
        lane_head = lax.div(iota((2 * c.own, tile), 1), c.size)
        reads = None
        for h in range(c.per_tile):
            wide = dot(both, s.spread[h]).astype(BF16)
            lhs = jnp.concatenate([wide * s.mask[g] for g in range(c.groups)], axis=1)
            part = dot(lhs, s.states16[l, :, at])
            reads = part if reads is None else jnp.where(lane_head == h, part, reads)
        step = lambda x, t: x[t * c.own_seqs : (t + 1) * c.own_seqs]
        rk = reads[: c.own]
        rq = reads[c.own :]
        dec = s.dec[:, at]
        beta = s.beta[:, at]
        names, prods = [], []
        for t in range(c.slots):
            for i in range(t + 1):
                names.append(("q", i, t))
                prods.append(step(k, i) * step(q, t))
                if i < t:
                    names.append(("k", i, t))
                    prods.append(step(k, i) * step(k, t))
        pairs = dot(jnp.concatenate(prods, axis=0).astype(BF16), s.blocks[...])
        pairs = {name: step(pairs, i) for i, name in enumerate(names)}
        fresh, outs = [], []
        whole = None
        for t in range(c.slots):
            g = step(dec, t)
            whole = g if whole is None else whole * g
            fresh = [(u * g) for u in fresh]
            guess = whole * step(rk, t)
            for i in range(t):
                guess = guess + pairs["k", i, t] * fresh[i]
            fresh.append(step(beta, t) * (step(v, t) - guess))
            o = whole * step(rq, t)
            for i in range(t + 1):
                o = o + pairs["q", i, t] * fresh[i]
            outs.append(o)
        wx[l, :, at] = jnp.concatenate(fresh, axis=0).astype(BF16)
        gx[l, :, at] = whole
        o = jnp.concatenate(outs, axis=0)
        total = dot((o * o).astype(BF16), s.blocks[...])
        o = o * lax.rsqrt(total / c.size + EPS) * s.gain[l, :1] * zed
        s.y[l, j, me] = dot(s.place[...], o.astype(BF16)).astype(BF16)
        for d in range(chips - 1):
            y_far(l, j, d).start()
        y_near(l, j, 0).start()

    def y_far(l, j, d):
        return remote(s.y.at[l, j, me], s.y.at[l, j, me], s.yf_s.at[l, j, d], s.yf_r.at[l, j, d], "dp", others[d])

    def y_near(l, j, d):
        source = me if d == 0 else sources[d - 1]
        return remote(
            s.y.at[l, j, source], s.y.at[l, j, source], s.yn_s.at[l, j, d], s.yn_r.at[l, j, d], "dp", partner
        )

    def forward(l, j):
        for d in range(chips - 1):
            y_far(l, j, d).wait()
            y_near(l, j, d + 1).start()

    def gather(l, j):
        for d in range(chips):
            y_near(l, j, d).wait()
        at = slice(j * tile, (j + 1) * tile)
        s.gated[:, at] = jnp.zeros((c.packed, tile), BF16)
        for d in range(n):
            here = slice(d * c.own_seqs, d * c.own_seqs + c.win)
            s.gated[here, at] = s.gated[here, at] + s.y[l, j, d]

    def inward(l, p):
        return remote(s.sent.at[l, p], s.came.at[l, p], s.in_s.at[l, p], s.in_r.at[l, p], "tp", toward)

    def across(l, p):
        return remote(s.sent.at[l, p], s.over.at[l, p], s.over_s.at[l, p], s.over_r.at[l, p], "tp", toward)

    def outward(l, p):
        return remote(s.full.at[l, p], s.full.at[l, p], s.full_s.at[l, p], s.full_r.at[l, p], "tp", away)

    def mix_out(l, p):
        at = slice(p * c.part, (p + 1) * c.part)
        s.sent[l, p] = dot(s.gated[...], s.wo[l, :, at]).astype(BF16)
        if half > 1:

            @pl.when(depth > 0)
            def _():
                inward(l, p).wait_recv()
                s.sent[l, p] = (s.sent[l, p].astype(F32) + s.came[l, p].astype(F32)).astype(BF16)

        @pl.when(centre)
        def _():
            across(l, p).start()

        if half > 1:

            @pl.when(jnp.logical_not(centre))
            def _():
                inward(l, p).start()

    def mix_in(l, p):
        @pl.when(centre)
        def _():
            across(l, p).wait_recv()
            s.full[l, p] = (s.sent[l, p].astype(F32) + s.over[l, p].astype(F32)).astype(BF16)

        if half > 1:

            @pl.when(jnp.logical_not(centre))
            def _():
                outward(l, p).wait_recv()

            @pl.when(depth > 0)
            def _():
                outward(l, p).start()

        at = slice(p * c.part, (p + 1) * c.part)
        new = (s.h[:, at] + s.full[l, p].astype(F32)).astype(BF16)
        if l + 1 == BLOCKS:
            hx[:, at] = new
        else:
            s.h[:, at] = new.astype(F32)
            s.scaled[l + 1, :, at] = (new.astype(F32) * s.scaling[...].astype(F32)[l + 1 : l + 2, at]).astype(BF16)

    def mix_end(l):
        for p in range(c.parts):

            @pl.when(centre)
            def _():
                across(l, p).wait_send()

            if half > 1:

                @pl.when(jnp.logical_not(centre))
                def _():
                    inward(l, p).wait_send()

                @pl.when(depth > 0)
                def _():
                    outward(l, p).wait_send()

    def setup():
        r = iota((c.own, c.lanes), 0)
        pos, live = columns(c.own, lax.rem(r, c.own_seqs) + me * c.own_seqs, lax.div(r, c.own_seqs))
        offset = (iota((c.own, c.win), 1) + me * c.own_seqs).astype(F32)
        s.pick[...] = jnp.where((offset == pos) & live, 1.0, 0.0).astype(BF16)
        s.live[...] = jnp.broadcast_to(jnp.where(live, 1.0, 0.0), s.live.shape)
        shape = (c.lanes, c.own)
        pos, live = rows_of(
            lax.rem(iota(shape, 1), c.own_seqs) + me * c.own_seqs, lax.div(iota(shape, 1), c.own_seqs)
        )
        offset = (iota((c.win, c.own), 0) + me * c.own_seqs).astype(F32)
        s.place[...] = jnp.where((offset == pos) & live, 1.0, 0.0).astype(BF16)
        r = iota((c.rows, c.lanes), 0)
        pos, live = columns(c.rows, lax.div(r, c.slots), lax.rem(r, c.slots))
        offset = iota((c.rows, c.packed), 1).astype(F32)
        hot[...] = jnp.where((offset == pos) & live, 1.0, 0.0).astype(BF16)
        fold = (iota((c.size, tile), 0) == lax.rem(iota((c.size, tile), 1), c.size)).astype(BF16)
        for l in range(BLOCKS):
            channels = jnp.broadcast_to(s.channel[...].astype(F32)[l : l + 1], (8, c.size)).astype(BF16)
            s.gain[l] = dot(channels, fold)

    def round_states(l):
        state_loads[l].wait()
        for i in range(c.own_seqs):
            s.states16[l, i * c.size : (i + 1) * c.size] = s.states[l, i].astype(BF16)

    for l in range(BLOCKS):
        acc = None
        if l:
            for p in range(c.parts):
                mix_in(l - 1, p)
                at = slice(p * c.part, (p + 1) * c.part)
                piece = s.scaled[l, :, at]
                if p == 0:
                    for j in range(c.chunks):
                        for i in range(4):
                            w_loads[l, j, i].wait()
                last = p + 1 == c.parts
                if not last:
                    for j in range(c.chunks):
                        for i in range(4):
                            val = dot(piece, s.w[l, i, at, j * tile : (j + 1) * tile])
                            s.acc[j, i] = val if p == 0 else s.acc[j, i] + val

            def acc(j, i, piece=piece, at=at, l=l):
                return s.acc[j, i] + dot(piece, s.w[l, i, at, j * tile : (j + 1) * tile])

        produce(l, 0, acc)
        produce_small(l)
        for j in range(1, c.chunks):
            produce(l, j, acc)
            if j == 1:
                cross(l, 0)
            elif j == 2:
                cross(l, -1)
        for j in ([] if c.chunks > 2 else [-1]) + list(range(0 if c.chunks == 1 else 1, c.chunks)):
            cross(l, j)
        if l == 0:
            load_weights(1)
            load_rest(1)
            setup()
            round_states(0)
        finish(l, -1)
        prepare(l)
        finish(l, 0)
        for j in range(1, c.chunks):
            finish(l, j)
            recur(l, j - 1)
        if l:
            mix_end(l - 1)
        recur(l, c.chunks - 1)
        for j in range(c.chunks):
            forward(l, j)
        wo_loads[l].wait()
        for j in range(c.chunks):
            gather(l, j)
        for p in range(c.parts):
            mix_out(l, p)
        if l == 0:
            round_states(1)
    for p in range(c.parts):
        mix_in(BLOCKS - 1, p)
    mix_end(BLOCKS - 1)


def run_main(c, args):
    ab = 2 * args[6].shape[2]
    half = 2 * c.tile
    chips, n = c.chips, c.n
    dma = lambda *shape: pltpu.SemaphoreType.DMA(shape)
    buf = lambda *shape: pltpu.VMEM(shape, BF16)
    wide = lambda *shape: pltpu.VMEM(shape, F32)
    every = 1 + c.chunks
    scratch = dict(
        flat=buf(c.rows, c.feat),
        scaling=buf(BLOCKS, c.feat),
        wa=buf(BLOCKS, c.feat, ab // 2),
        wb=buf(BLOCKS, c.feat, ab // 2),
        wab=buf(BLOCKS, c.feat, ab),
        speed=wide(BLOCKS, c.heads),
        bias=wide(BLOCKS, c.heads),
        channel=buf(BLOCKS, c.size),
        shrink=wide(BLOCKS, c.own_seqs, c.slots, c.heads),
        w=buf(BLOCKS, 4, c.feat, c.cols),
        wo=buf(BLOCKS, c.cols, c.feat),
        states=wide(BLOCKS, c.own_seqs, c.size, c.cols),
        states16=buf(BLOCKS, c.own_seqs * c.size, c.cols),
        counts=pltpu.VMEM((n, 8, c.lanes), jnp.int32),
        blocks=buf(c.tile, c.tile),
        spread=buf(c.per_tile, c.tile, c.tile),
        mask=buf(c.groups, 2 * c.own, c.tile),
        gain=wide(BLOCKS, 8, c.tile),
        pick=buf(c.own, c.win),
        place=buf(c.win, c.own),
        live=wide(c.own, 128),
        factor=wide(c.own, 128),
        dec=wide(c.own, c.cols),
        beta=wide(c.own, c.cols),
        h=wide(c.packed, c.feat),
        scaled=buf(BLOCKS, c.packed, c.feat),
        acc=wide(c.chunks, 4, c.packed, c.tile),
        x=buf(BLOCKS, c.chunks, 2, c.packed, half),
        pair=buf(BLOCKS, c.chunks, c.packed, half),
        sum=buf(BLOCKS, c.chunks, c.packed, half),
        far=buf(BLOCKS, c.chunks, chips - 1, c.chip_win, half),
        out=buf(BLOCKS, c.chunks, c.win, half),
        fin=buf(BLOCKS, c.chunks, 2, c.win, half),
        x_small=buf(BLOCKS, 2, c.packed, ab),
        pair_small=buf(BLOCKS, c.packed, ab),
        sum_small=buf(BLOCKS, c.packed, ab),
        far_small=buf(BLOCKS, chips - 1, c.chip_win, ab),
        out_small=buf(BLOCKS, c.win, ab),
        fin_small=buf(BLOCKS, 2, c.win, ab),
        y=buf(BLOCKS, c.chunks, n, c.win, c.tile),
        gated=buf(c.packed, c.cols),
        sent=buf(BLOCKS, c.parts, c.packed, c.part),
        came=buf(BLOCKS, c.parts, c.packed, c.part),
        over=buf(BLOCKS, c.parts, c.packed, c.part),
        full=buf(BLOCKS, c.parts, c.packed, c.part),
        small_sem=dma(8),
        w_sem=dma(BLOCKS, c.chunks, 4),
        wo_sem=dma(BLOCKS),
        state_sem=dma(BLOCKS),
        count_s=dma(n - 1),
        count_r=dma(n - 1),
        first_s=dma(BLOCKS, every),
        first_r=dma(BLOCKS, every),
        second_s=dma(BLOCKS, every, chips - 1),
        second_r=dma(BLOCKS, every, chips - 1),
        third_s=dma(BLOCKS, every),
        third_r=dma(BLOCKS, every),
        yf_s=dma(BLOCKS, c.chunks, chips - 1),
        yf_r=dma(BLOCKS, c.chunks, chips - 1),
        yn_s=dma(BLOCKS, c.chunks, chips),
        yn_r=dma(BLOCKS, c.chunks, chips),
        in_s=dma(BLOCKS, c.parts),
        in_r=dma(BLOCKS, c.parts),
        over_s=dma(BLOCKS, c.parts),
        over_r=dma(BLOCKS, c.parts),
        full_s=dma(BLOCKS, c.parts),
        full_r=dma(BLOCKS, c.parts),
    )
    c.names = list(scratch)
    return pl.pallas_call(
        functools.partial(main_kernel, c),
        out_shape=[
            jax.ShapeDtypeStruct((BLOCKS, c.own, c.cols), BF16),
            jax.ShapeDtypeStruct((BLOCKS, c.own, c.cols), BF16),
            jax.ShapeDtypeStruct((BLOCKS, c.own_seqs, c.cols), F32),
            jax.ShapeDtypeStruct((c.packed, c.feat), BF16),
            jax.ShapeDtypeStruct((c.rows, c.packed), BF16),
        ],
        in_specs=[SMEM] + [HBM] * 14,
        out_specs=[VMEM] * 5,
        scratch_shapes=list(scratch.values()),
        compiler_params=pltpu.CompilerParams(
            collective_id=1, has_side_effects=True, vmem_limit_bytes=50 * 1024 * 1024
        ),
        name="blocks",
    )(*args)


def write_kernel(c, group, kx, wx, gx, hx, hot, flat, states, new, tokens, keys, fresh):
    step = pl.program_id(1)
    tile = c.tile
    row_head = lax.div(iota((c.per_tile * c.own, tile), 0), c.own)
    lane_head = lax.div(iota((c.per_tile * c.own, tile), 1), c.size)
    same = (row_head == lane_head).astype(BF16)

    @pl.when((step == 0) & (pl.program_id(0) == 0))
    def _():
        live = hot[...]
        back = dot(live, hx[...])
        count = jnp.sum(live.astype(F32), axis=1, keepdims=True)
        tokens[...] = jnp.where(count > 0.0, back, flat[...].astype(F32)).astype(BF16)

    @pl.when(step == 0)
    def _():
        fold = (iota((c.size, tile), 0) == lax.rem(iota((c.size, tile), 1), c.size)).astype(BF16)
        for j in range(c.chunks):
            at = slice(j * tile, (j + 1) * tile)
            keys[j] = lax.dot_general(
                fold, tiles(kx[0, :, at], c.per_tile) * same, (((1,), (1,)), ((), ())),
                preferred_element_type=F32,
            ).astype(BF16)
            fresh[j] = tiles(wx[0, :, at], c.per_tile) * same

    shape = (c.size, c.per_tile * c.own)
    owner = lax.rem(iota(shape, 1), c.own_seqs)
    for j in range(c.chunks):
        at = slice(j * tile, (j + 1) * tile)
        lhs = jnp.concatenate(
            [keys[j] * (owner == step * group + i).astype(BF16) for i in range(group)], axis=0
        )
        added = dot(lhs, fresh[j])
        for i in range(group):
            decay = gx[0, pl.ds(step * group + i, 1), at]
            new[0, i, :, at] = states[0, i, :, at] * decay + added[i * c.size : (i + 1) * c.size]


def run_write(c, kx, wx, gx, hx, hot, flat, states):
    group = 4
    layer = lambda a: pl.BlockSpec((1,) + a.shape[1:], lambda l, g: (l, 0, 0))
    whole = lambda a: pl.BlockSpec(a.shape, lambda l, g: (0, 0))
    block = pl.BlockSpec((1, group) + states.shape[2:], lambda l, g: (l, g, 0, 0))
    return pl.pallas_call(
        functools.partial(write_kernel, c, group),
        out_shape=[
            jax.ShapeDtypeStruct(states.shape, F32),
            jax.ShapeDtypeStruct(flat.shape, BF16),
        ],
        grid=(BLOCKS, c.own_seqs // group),
        in_specs=[layer(kx), layer(wx), layer(gx), whole(hx), whole(hot), whole(flat), block],
        out_specs=[block, whole(flat)],
        scratch_shapes=[
            pltpu.VMEM((c.chunks, c.size, c.per_tile * c.own), BF16),
            pltpu.VMEM((c.chunks, c.per_tile * c.own, c.tile), BF16),
        ],
        name="write",
    )(kx, wx, gx, hx, hot, flat, states)


def body(
    n, m, resid, counts, wq, wk, wv, wz, wa, wb, wo, speed, bias, scaling, channel, shrink, states,
):
    c = sizes(n, m, resid, counts, wq, speed)
    flat = resid.reshape(c.rows, c.feat)
    outs = run_main(
        c, (counts, flat, wq, wk, wv, wz, wa, wb, wo, speed, bias, scaling, channel, shrink, states)
    )
    new, tokens = run_write(c, *outs, flat, states)
    return tokens.reshape(resid.shape), new


def solution(mesh):
    in_specs = (
        P("grp", None, "dp"),
        P(("grp", "dp")),
        P(None, "dp", "tp"),
        P(None, "dp", "tp"),
        P(None, "dp", "tp"),
        P(None, "dp", "tp"),
        P(),
        P(),
        P(None, "tp", "dp"),
        P(None, "tp"),
        P(None, "tp"),
        P(None, "dp"),
        P(),
        P(None, ("grp", "dp"), None, "tp"),
        P(None, ("grp", "dp"), None, "tp"),
    )
    out_specs = (P("grp", None, "dp"), P(None, ("grp", "dp"), None, "tp"))
    run = functools.partial(body, mesh.shape["dp"], mesh.shape["tp"])
    return jax.shard_map(run, mesh=mesh, in_specs=in_specs, out_specs=out_specs, check_vma=False)
```

time: 129 us -> 96.6 us (0.75)
  Pallas kernels: 107 us -> 83.8 us
  local copies, waits for them, and re-layouts: 18.6 us -> 11.6 us
    pallas_call x7 -> x2, Pallas kernels: 107 us -> 83.8 us  [the longest x1 72.4 us: run_main(): pl.pallas_call(functools.partial(main_kernel, c), out_shape=[jax.ShapeDty...]
    unnamed x36 -> x26, local copies, waits for them, and re-layouts: 12.3 us -> 8.38 us
    reshape x2, local copies, waits for them, and re-layouts: 1.11 us -> 3.24 us  [the longest x1 2.03 us: body(): return (tokens.reshape(resid.shape), new)]
    another operation x4 -> x0, local copies, waits for them, and re-layouts: 1.34 us -> none  [body(): gain = jnp.tile(channel[l].astype(F32), heads)[None]]
    broadcast_in_dim x3 -> x0, local copies, waits for them, and re-layouts: 1.3 us -> none  [the longest x2 1.29 us: recur(): args = [main, small, pos[:, None], pos[None, :], speed, bias, shrink, gain]]
where the time goes in v1:
time: 96.6 us; the launch traced here: 96.1 us
  Pallas kernels  83.8 us (87%)
  local copies, waits for them, and re-layouts  11.6 us (12%)
    pallas_call x1, Pallas kernels, run_main(): pl.pallas_call(functools.partial(main_kernel, c), out_shape=[jax.ShapeDty...  72.4 us
    pallas_call x1, Pallas kernels, run_write(): pl.pallas_call(functools.partial(write_kernel, c, group), out_shape=[jax....  11.4 us
    unnamed x26, local copies, waits for them, and re-layouts  8.38 us
    reshape x1, local copies, waits for them, and re-layouts, body(): return (tokens.reshape(resid.shape), new)  2.03 us

profile of v1, /device:TPU:0, one launch (start us, length us, event | category | flops | bytes accessed | tf_op | source)
XLA Modules:
  0.0 96.1 jit_solution(1047999059471051991)
XLA Ops:
  0.6 0.0 copy-start.5
  0.6 0.0 copy-start.11
  0.7 0.0 copy-start.7
  0.7 0.0 copy-start.9
  0.7 0.0 copy-start.8
  0.7 0.0 copy-start.10
  0.7 1.2 %reshape.10.flat = bf16[256,1024]{1,0:T(8,128)(2,1)S(1)} reshape(bf16[64,4,1024]{2,1,0:T(4,128)(2,1)} %param.15) | data formatting | bytes 1048576 | tf_op jit(solution)/shard_map/reshape | solution.py:670
  1.9 0.0 copy-start
  1.9 2.3 %copy.17.wa = bf16[2,4096,64]{2,1,0:T(8,128)(2,1)S(1)} copy(bf16[2,4096,64]{1,2,0:T(8,128)(2,1)} %param.21) | data formatting | bytes 2097152 | tf_op args[6]
  4.2 2.7 %copy.18.wb = bf16[2,4096,64]{2,1,0:T(8,128)(2,1)} copy(bf16[2,4096,64]{1,2,0:T(8,128)(2,1)} %param.22) | data formatting | bytes 2097152 | tf_op args[7]
  6.9 0.0 copy-done.5
  6.9 0.0 copy-done.11
  6.9 0.0 copy-done.7
  6.9 0.0 copy-done.9
  7.0 0.0 copy-done.8
  7.0 0.0 copy-done.10
  7.0 72.4 %blocks.1 = (bf16[2,64,1024]{2,1,0:T(8,128)(2,1)S(1)}, bf16[2,64,1024]{2,1,0:T(8,128)(2,1)S(1)}, f32[2,16,1024]{2,1,0:T(8,128)S(1)}, bf16[96,1024]{1,0:T(8,128)(2,1)S(1)}, bf16[256,96]{1,0:T(8,128)(2,1)S(1)}) custom-call(s32[16]{0:T(128)S(1)} %copy-done.10, bf16[256,1024]{1,0:T(8,128)(2,1)S(1)} %reshape.10.flat, bf16[2,1024,1024]{2,1,0:T(8,128)(2,1)} %wq.1, ...), custom_call_target="tpu_custom_call" | custom-call | tf_op jit(solution)/shard_map/blocks/pallas_call | solution.py:587
  79.4 0.0 copy-done
  79.4 0.0 copy-start.1
  79.4 0.7 copy-done.1
  80.1 0.0 copy-start.2
  80.1 0.7 copy-done.2
  80.8 0.0 copy-start.3
  80.8 0.7 copy-done.3
  81.5 0.0 copy-start.4
  81.5 0.6 copy-done.4
  82.1 0.0 copy-start.6
  82.1 0.6 copy-done.6
  82.7 11.4 %write.1 = (f32[2,16,64,1024]{3,2,1,0:T(8,128)}, bf16[256,1024]{1,0:T(8,128)(2,1)}) custom-call(bf16[2,64,1024]{2,1,0:T(8,128)(2,1)} %copy-done.1, bf16[2,64,1024]{2,1,0:T(8,128)(2,1)} %copy-done.2, f32[2,16,1024]{2,1,0:T(8,128)} %copy-done.4, bf16[96,1024]{1,0:T(8,128)(2,1)} %copy-done.3, bf16[256,96]{1,0:T(8,128)(2,1)} %copy-done.6, ...), custom_call_target="tpu_custom_call" | custom-call | tf_op jit(solution)/shard_map/write/pallas_call | solution.py:649
  94.1 2.0 %reshape.11 = bf16[64,4,1024]{2,1,0:T(4,128)(2,1)} reshape(bf16[256,1024]{1,0:T(8,128)(2,1)} %get-tuple-element.14) | data formatting | bytes 1048576 | tf_op jit(solution)/shard_map/reshape | solution.py:675
Async XLA Ops:
  0.6 6.3 %copy-start.5 = (f32[2,16,4,16]{3,2,1,0:T(4,128)S(1)}, f32[2,16,4,16]{3,2,1,0:T(4,128)}, u32[]{:S(2)}) copy-start(f32[2,16,4,16]{3,2,1,0:T(4,128)} %shrink.1) | copy-start | bytes 24580
  0.6 6.3 %copy-start.11 = (bf16[2,64]{1,0:T(2,128)(2,1)S(1)}, bf16[2,64]{1,0:T(2,128)(2,1)}, u32[]{:S(2)}) copy-start(bf16[2,64]{1,0:T(2,128)(2,1)} %channel.1) | copy-start | bytes 772
  0.7 6.3 %copy-start.7 = (bf16[2,1024]{1,0:T(2,128)(2,1)S(1)}, bf16[2,1024]{1,0:T(2,128)(2,1)}, u32[]{:S(2)}) copy-start(bf16[2,1024]{1,0:T(2,128)(2,1)} %scaling.1) | copy-start | bytes 12292
  0.7 6.3 %copy-start.9 = (f32[2,16]{1,0:T(2,128)S(1)}, f32[2,16]{1,0:T(2,128)}, u32[]{:S(2)}) copy-start(f32[2,16]{1,0:T(2,128)} %bias.1) | copy-start | bytes 388
  0.7 6.3 %copy-start.8 = (f32[2,16]{1,0:T(2,128)S(1)}, f32[2,16]{1,0:T(2,128)}, u32[]{:S(2)}) copy-start(f32[2,16]{1,0:T(2,128)} %speed.1) | copy-start | bytes 388
  0.7 6.3 %copy-start.10 = (s32[16]{0:T(128)S(1)}, s32[16]{0:T(128)}, u32[]{:S(2)}) copy-start(s32[16]{0:T(128)} %counts.1) | copy-start | bytes 196
  1.9 77.5 %copy-start = (bf16[256,1024]{1,0:T(8,128)(2,1)}, bf16[256,1024]{1,0:T(8,128)(2,1)S(1)}, u32[]{:S(2)}) copy-start(bf16[256,1024]{1,0:T(8,128)(2,1)S(1)} %reshape.10.flat) | copy-start | bytes 1572868
  79.4 0.7 copy-start.1
  80.1 0.7 copy-start.2
  80.8 0.7 copy-start.3
  81.5 0.6 copy-start.4
  82.1 0.6 copy-start.6

commit v2 on v1

--- a/solution.py
+++ b/solution.py
@@ -59,8 +59,8 @@
 
 
 def main_kernel(
-    c, counts, flat, wq, wk, wv, wz, wa, wb, wo, speed, bias, scaling, channel, shrink, states,
-    kx, wx, gx, hx, hot, *scratch,
+    c, counts, resid, wq, wk, wv, wz, wa, wb, wo, speed, bias, scaling, channel, shrink, states,
+    tokens, new, *scratch,
 ):
     s = types.SimpleNamespace(**dict(zip(c.names, scratch)))
     n, m, chips, tile = c.n, c.m, c.chips, c.tile
@@ -89,12 +89,16 @@
         copy.start()
         return copy
 
-    feats = pl.ds(pl.multiple_of(me * c.feat, 16), c.feat)
+    all_heads = wa.shape[1]
+    ab = 2 * all_heads
+    feats = pl.ds(pl.multiple_of(me * c.feat, 128), c.feat)
     early = [
         load(src, dst, s.small_sem.at[i])
         for i, (src, dst) in enumerate(
             [
-                (flat, s.flat), (scaling, s.scaling), (wa.at[:, feats, :], s.wa), (wb.at[:, feats, :], s.wb),
+                (resid, s.resid), (scaling, s.scaling),
+                (wa.at[:, :, feats], s.wab.at[:, pl.ds(0, all_heads)]),
+                (wb.at[:, :, feats], s.wab.at[:, pl.ds(all_heads, all_heads)]),
                 (speed, s.speed), (bias, s.bias), (channel, s.channel), (shrink, s.shrink),
             ]
         )
@@ -108,7 +112,7 @@
                 w_loads[l, j, i] = load(w.at[l, :, at], s.w.at[l, i, :, at], s.w_sem.at[l, j, i])
 
     def load_rest(l):
-        state_loads[l] = load(states.at[l], s.states.at[l], s.state_sem.at[l])
+        state_loads[l] = load(states.at[l], new.at[l], s.state_sem.at[l])
         wo_loads[l] = load(wo.at[l], s.wo.at[l], s.wo_sem.at[l])
 
     load_weights(0)
@@ -146,12 +150,6 @@
     load_rest(0)
     for copy in early:
         copy.wait()
-    all_heads = wa.shape[2]
-    ab = 2 * all_heads
-    for l in range(BLOCKS):
-        at_a = (iota((all_heads, ab), 0) == iota((all_heads, ab), 1)).astype(BF16)
-        at_b = (iota((all_heads, ab), 0) + all_heads == iota((all_heads, ab), 1)).astype(BF16)
-        s.wab[l] = (dot(s.wa[l], at_a) + dot(s.wb[l], at_b)).astype(BF16)
 
     for copy in swaps:
         copy.wait()
@@ -179,7 +177,7 @@
     shape = (c.lanes, c.rows)
     pos, live = rows_of(lax.div(iota(shape, 1), c.slots), lax.rem(iota(shape, 1), c.slots))
     into = jnp.where((iota((c.packed, c.rows), 0).astype(F32) == pos) & live, 1.0, 0.0).astype(BF16)
-    h0 = dot(into, s.flat[...])
+    h0 = dot(into, s.resid[...].reshape(c.rows, c.feat))
     s.h[...] = h0
     s.scaled[0] = (h0 * s.scaling[...].astype(F32)[:1]).astype(BF16)
 
@@ -195,7 +193,9 @@
 
     def produce_small(l):
         h = s.h[...]
-        s.x_small[l, 0] = dot(s.scaled[l], s.wab[l]).astype(BF16)
+        s.x_small[l, 0] = lax.dot_general(
+            s.scaled[l], s.wab[l], (((1,), (1,)), ((), ())), preferred_element_type=F32
+        ).astype(BF16)
         squares = jnp.sum(h * h, axis=1, keepdims=True)
         s.x_small[l, 1] = jnp.broadcast_to(squares, (c.packed, ab)).astype(BF16)
         first(l, -1).start()
@@ -281,7 +281,7 @@
             kept.append(val)
         q, k, v, zed = kept
         both = jnp.concatenate([k, q], axis=0).astype(BF16)
-        kx[l, :, at] = both[: c.own]
+        s.k[l, :, at] = both[: c.own]
         lane_head = lax.div(iota((2 * c.own, tile), 1), c.size)
         reads = None
         for h in range(c.per_tile):
@@ -318,8 +318,8 @@
             for i in range(t + 1):
                 o = o + pairs["q", i, t] * fresh[i]
             outs.append(o)
-        wx[l, :, at] = jnp.concatenate(fresh, axis=0).astype(BF16)
-        gx[l, :, at] = whole
+        s.u[l, :, at] = jnp.concatenate(fresh, axis=0).astype(BF16)
+        s.decay[l, :, at] = whole
         o = jnp.concatenate(outs, axis=0)
         total = dot((o * o).astype(BF16), s.blocks[...])
         o = o * lax.rsqrt(total / c.size + EPS) * s.gain[l, :1] * zed
@@ -397,12 +397,12 @@
                 outward(l, p).start()
 
         at = slice(p * c.part, (p + 1) * c.part)
-        new = (s.h[:, at] + s.full[l, p].astype(F32)).astype(BF16)
+        mixed = (s.h[:, at] + s.full[l, p].astype(F32)).astype(BF16)
         if l + 1 == BLOCKS:
-            hx[:, at] = new
+            s.last[:, at] = mixed
         else:
-            s.h[:, at] = new.astype(F32)
-            s.scaled[l + 1, :, at] = (new.astype(F32) * s.scaling[...].astype(F32)[l + 1 : l + 2, at]).astype(BF16)
+            s.h[:, at] = mixed.astype(F32)
+            s.scaled[l + 1, :, at] = (mixed.astype(F32) * s.scaling[...].astype(F32)[l + 1 : l + 2, at]).astype(BF16)
 
     def mix_end(l):
         for p in range(c.parts):
@@ -436,16 +436,39 @@
         r = iota((c.rows, c.lanes), 0)
         pos, live = columns(c.rows, lax.div(r, c.slots), lax.rem(r, c.slots))
         offset = iota((c.rows, c.packed), 1).astype(F32)
-        hot[...] = jnp.where((offset == pos) & live, 1.0, 0.0).astype(BF16)
+        s.hot[...] = jnp.where((offset == pos) & live, 1.0, 0.0).astype(BF16)
+        s.alive[...] = jnp.broadcast_to(jnp.where(live, 1.0, 0.0), s.alive.shape)
         fold = (iota((c.size, tile), 0) == lax.rem(iota((c.size, tile), 1), c.size)).astype(BF16)
         for l in range(BLOCKS):
             channels = jnp.broadcast_to(s.channel[...].astype(F32)[l : l + 1], (8, c.size)).astype(BF16)
             s.gain[l] = dot(channels, fold)
 
+    def write_states(l, j):
+        at = slice(j * tile, (j + 1) * tile)
+        shape = (c.per_tile * c.own, tile)
+        same = (lax.div(iota(shape, 0), c.own) == lax.div(iota(shape, 1), c.size)).astype(BF16)
+        fold = (iota((c.size, tile), 0) == lax.rem(iota((c.size, tile), 1), c.size)).astype(BF16)
+        keys = lax.dot_general(
+            fold, tiles(s.k[l, :, at], c.per_tile) * same, (((1,), (1,)), ((), ())), preferred_element_type=F32
+        ).astype(BF16)
+        fresh = tiles(s.u[l, :, at], c.per_tile) * same
+        owner = lax.rem(iota((c.size, c.per_tile * c.own), 1), c.own_seqs)
+        batch = 4
+        for first_seq in range(0, c.own_seqs, batch):
+            lhs = jnp.concatenate(
+                [keys * (owner == first_seq + i).astype(BF16) for i in range(batch)], axis=0
+            )
+            added = dot(lhs, fresh)
+            for i in range(batch):
+                seq = first_seq + i
+                new[l, seq, :, at] = (
+                    new[l, seq, :, at] * s.decay[l, seq : seq + 1, at] + added[i * c.size : (i + 1) * c.size]
+                )
+
     def round_states(l):
         state_loads[l].wait()
         for i in range(c.own_seqs):
-            s.states16[l, i * c.size : (i + 1) * c.size] = s.states[l, i].astype(BF16)
+            s.states16[l, i * c.size : (i + 1) * c.size] = new[l, i].astype(BF16)
 
     for l in range(BLOCKS):
         acc = None
@@ -499,15 +522,20 @@
             gather(l, j)
         for p in range(c.parts):
             mix_out(l, p)
+        for j in range(c.chunks):
+            write_states(l, j)
         if l == 0:
             round_states(1)
     for p in range(c.parts):
         mix_in(BLOCKS - 1, p)
+    back = dot(s.hot[...], s.last[...])
+    old = s.resid[...].reshape(c.rows, c.feat).astype(F32)
+    tokens[...] = jnp.where(s.alive[:, :1] > 0.0, back, old).astype(BF16).reshape(tokens.shape)
     mix_end(BLOCKS - 1)
 
 
 def run_main(c, args):
-    ab = 2 * args[6].shape[2]
+    ab = 2 * args[6].shape[1]
     half = 2 * c.tile
     chips, n = c.chips, c.n
     dma = lambda *shape: pltpu.SemaphoreType.DMA(shape)
@@ -515,18 +543,21 @@
     wide = lambda *shape: pltpu.VMEM(shape, F32)
     every = 1 + c.chunks
     scratch = dict(
-        flat=buf(c.rows, c.feat),
+        resid=buf(c.seqs, c.slots, c.feat),
+        last=buf(c.packed, c.feat),
+        hot=buf(c.rows, c.packed),
+        alive=wide(c.rows, 128),
+        k=buf(BLOCKS, c.own, c.cols),
+        u=buf(BLOCKS, c.own, c.cols),
+        decay=wide(BLOCKS, c.own_seqs, c.cols),
         scaling=buf(BLOCKS, c.feat),
-        wa=buf(BLOCKS, c.feat, ab // 2),
-        wb=buf(BLOCKS, c.feat, ab // 2),
-        wab=buf(BLOCKS, c.feat, ab),
+        wab=buf(BLOCKS, ab, c.feat),
         speed=wide(BLOCKS, c.heads),
         bias=wide(BLOCKS, c.heads),
         channel=buf(BLOCKS, c.size),
         shrink=wide(BLOCKS, c.own_seqs, c.slots, c.heads),
         w=buf(BLOCKS, 4, c.feat, c.cols),
         wo=buf(BLOCKS, c.cols, c.feat),
-        states=wide(BLOCKS, c.own_seqs, c.size, c.cols),
         states16=buf(BLOCKS, c.own_seqs * c.size, c.cols),
         counts=pltpu.VMEM((n, 8, c.lanes), jnp.int32),
         blocks=buf(c.tile, c.tile),
@@ -587,92 +618,28 @@
     return pl.pallas_call(
         functools.partial(main_kernel, c),
         out_shape=[
-            jax.ShapeDtypeStruct((BLOCKS, c.own, c.cols), BF16),
-            jax.ShapeDtypeStruct((BLOCKS, c.own, c.cols), BF16),
-            jax.ShapeDtypeStruct((BLOCKS, c.own_seqs, c.cols), F32),
-            jax.ShapeDtypeStruct((c.packed, c.feat), BF16),
-            jax.ShapeDtypeStruct((c.rows, c.packed), BF16),
+            pltpu.VMEM(args[1].shape, BF16),
+            pltpu.VMEM(args[-1].shape, F32),
         ],
         in_specs=[SMEM] + [HBM] * 14,
-        out_specs=[VMEM] * 5,
+        out_specs=[VMEM] * 2,
         scratch_shapes=list(scratch.values()),
         compiler_params=pltpu.CompilerParams(
-            collective_id=1, has_side_effects=True, vmem_limit_bytes=50 * 1024 * 1024
+            collective_id=1, has_side_effects=True, vmem_limit_bytes=38 * 1024 * 1024
         ),
         name="blocks",
-    )(*args)
-
-
-def write_kernel(c, group, kx, wx, gx, hx, hot, flat, states, new, tokens, keys, fresh):
-    step = pl.program_id(1)
-    tile = c.tile
-    row_head = lax.div(iota((c.per_tile * c.own, tile), 0), c.own)
-    lane_head = lax.div(iota((c.per_tile * c.own, tile), 1), c.size)
-    same = (row_head == lane_head).astype(BF16)
-
-    @pl.when((step == 0) & (pl.program_id(0) == 0))
-    def _():
-        live = hot[...]
-        back = dot(live, hx[...])
-        count = jnp.sum(live.astype(F32), axis=1, keepdims=True)
-        tokens[...] = jnp.where(count > 0.0, back, flat[...].astype(F32)).astype(BF16)
-
-    @pl.when(step == 0)
-    def _():
-        fold = (iota((c.size, tile), 0) == lax.rem(iota((c.size, tile), 1), c.size)).astype(BF16)
-        for j in range(c.chunks):
-            at = slice(j * tile, (j + 1) * tile)
-            keys[j] = lax.dot_general(
-                fold, tiles(kx[0, :, at], c.per_tile) * same, (((1,), (1,)), ((), ())),
-                preferred_element_type=F32,
-            ).astype(BF16)
-            fresh[j] = tiles(wx[0, :, at], c.per_tile) * same
-
-    shape = (c.size, c.per_tile * c.own)
-    owner = lax.rem(iota(shape, 1), c.own_seqs)
-    for j in range(c.chunks):
-        at = slice(j * tile, (j + 1) * tile)
-        lhs = jnp.concatenate(
-            [keys[j] * (owner == step * group + i).astype(BF16) for i in range(group)], axis=0
-        )
-        added = dot(lhs, fresh[j])
-        for i in range(group):
-            decay = gx[0, pl.ds(step * group + i, 1), at]
-            new[0, i, :, at] = states[0, i, :, at] * decay + added[i * c.size : (i + 1) * c.size]
-
-
-def run_write(c, kx, wx, gx, hx, hot, flat, states):
-    group = 4
-    layer = lambda a: pl.BlockSpec((1,) + a.shape[1:], lambda l, g: (l, 0, 0))
-    whole = lambda a: pl.BlockSpec(a.shape, lambda l, g: (0, 0))
-    block = pl.BlockSpec((1, group) + states.shape[2:], lambda l, g: (l, g, 0, 0))
-    return pl.pallas_call(
-        functools.partial(write_kernel, c, group),
-        out_shape=[
-            jax.ShapeDtypeStruct(states.shape, F32),
-            jax.ShapeDtypeStruct(flat.shape, BF16),
-        ],
-        grid=(BLOCKS, c.own_seqs // group),
-        in_specs=[layer(kx), layer(wx), layer(gx), whole(hx), whole(hot), whole(flat), block],
-        out_specs=[block, whole(flat)],
-        scratch_shapes=[
-            pltpu.VMEM((c.chunks, c.size, c.per_tile * c.own), BF16),
-            pltpu.VMEM((c.chunks, c.per_tile * c.own, c.tile), BF16),
-        ],
-        name="write",
-    )(kx, wx, gx, hx, hot, flat, states)
+    )(*[args[0]] + [pltpu.with_memory_space_constraint(x, pltpu.HBM) for x in args[1:]])
 
 
 def body(
     n, m, resid, counts, wq, wk, wv, wz, wa, wb, wo, speed, bias, scaling, channel, shrink, states,
 ):
     c = sizes(n, m, resid, counts, wq, speed)
-    flat = resid.reshape(c.rows, c.feat)
-    outs = run_main(
-        c, (counts, flat, wq, wk, wv, wz, wa, wb, wo, speed, bias, scaling, channel, shrink, states)
+    turned = [jnp.swapaxes(w, 1, 2) for w in (wa, wb)]
+    tokens, new = run_main(
+        c, (counts, resid, wq, wk, wv, wz, *turned, wo, speed, bias, scaling, channel, shrink, states)
     )
-    new, tokens = run_write(c, *outs, flat, states)
-    return tokens.reshape(resid.shape), new
+    return tokens, new
 
 
 def solution(mesh):

time: 96.6 us -> 80.1 us (0.83)
  Pallas kernels: 83.8 us -> 74.4 us
  local copies, waits for them, and re-layouts: 11.6 us -> 4.84 us
    pallas_call x2 -> x1, Pallas kernels: 83.8 us -> 74.4 us  [run_main(): pl.pallas_call(functools.partial(main_kernel, c), out_shape=[pltpu.VMEM(a...]
    unnamed x26 -> x4, local copies, waits for them, and re-layouts: 8.38 us -> 4.84 us
    reshape x2 -> x0, local copies, waits for them, and re-layouts: 3.24 us -> none  [the longest x1 2.03 us: body(): return (tokens.reshape(resid.shape), new)]
where the time goes in v2:
time: 80.1 us; the launch traced here: 79.9 us
  Pallas kernels  74.4 us (93%)
  local copies, waits for them, and re-layouts  4.84 us (6%)
    pallas_call x1, Pallas kernels, run_main(): pl.pallas_call(functools.partial(main_kernel, c), out_shape=[pltpu.VMEM(a...  74.4 us
    unnamed x4, local copies, waits for them, and re-layouts  4.84 us

profile of v2, /device:TPU:0, one launch (start us, length us, event | category | flops | bytes accessed | tf_op | source)
XLA Modules:
  0.0 79.9 jit_solution(17445280219093979129)
XLA Ops:
  0.6 0.0 copy-start
  0.6 0.6 copy-done
  1.3 74.4 %blocks.1 = (bf16[64,4,1024]{2,1,0:T(4,128)(2,1)S(1)}, f32[2,16,64,1024]{3,2,1,0:T(8,128)S(1)}) custom-call(s32[16]{0:T(128)S(1)} %copy-done, bf16[64,4,1024]{2,1,0:T(4,128)(2,1)} %resid.1, bf16[2,1024,1024]{2,1,0:T(8,128)(2,1)} %wq.1, bf16[2,1024,1024]{2,1,0:T(8,128)(2,1)} %wk.1, bf16[2,1024,1024]{2,1,0:T(8,128)(2,1)} %wv.1, bf16[2,1024,1024]{2,1,0:T(8,128)(2,1)} %wz.1, ...), custom_call_target="tpu_custom_call" | custom-call | tf_op jit(solution)/shard_map/blocks/pallas_call | solution.py:618
  75.7 0.8 copy.19
  76.5 3.4 %copy.20 = f32[2,16,64,1024]{3,2,1,0:T(8,128)} copy(f32[2,16,64,1024]{3,2,1,0:T(8,128)S(1)} %get-tuple-element.3) | data formatting | bytes 16777216
Async XLA Ops:
  0.6 0.7 copy-start

commit v3 on v2

v3 whole, which is shorter than its diff:
```python
import functools
import types

import jax
import jax.numpy as jnp
from jax import lax
from jax.experimental import pallas as pl
from jax.experimental.pallas import tpu as pltpu
from jax.sharding import PartitionSpec as P

BLOCKS = 2
EPS = 1e-06
F32 = jnp.float32
BF16 = jnp.bfloat16
MESH = pl.DeviceIdType.MESH
VMEM = pl.BlockSpec(memory_space=pltpu.VMEM)
HBM = pl.BlockSpec(memory_space=pltpu.HBM)
SMEM = pl.BlockSpec(memory_space=pltpu.SMEM)


def iota(shape, dim):
    return lax.broadcasted_iota(jnp.int32, shape, dim)


def dot(a, b):
    return jnp.dot(a, b, preferred_element_type=F32)


def narrow(a, b):
    return lax.dot_general(a, b, (((1,), (1,)), ((), ())), preferred_element_type=F32)


def tiles(ref, count):
    return jnp.concatenate([ref] * count, axis=0)


def sizes(n, m, resid, counts, wq, speed):
    c = types.SimpleNamespace(n=n, m=m)
    c.seqs, c.slots, c.feat = resid.shape
    c.own_seqs = counts.shape[0]
    c.cols = wq.shape[2]
    c.heads = speed.shape[1]
    c.size = c.cols // c.heads
    c.own = c.own_seqs * c.slots
    c.rows = c.seqs * c.slots
    c.packed = c.seqs * 3 // 2
    c.chips = n // 2
    c.per_chip = 2 * c.own_seqs
    c.chip_win = c.packed - (c.chips - 1) * c.per_chip
    c.win = c.packed - (n - 1) * c.own_seqs
    c.tile = min(256, c.cols)
    c.chunks = c.cols // c.tile
    c.per_tile = c.tile // c.size
    c.groups = c.own_seqs // c.per_tile
    c.parts = 8
    c.pairs = c.parts // 2
    c.part = c.feat // c.parts
    c.lanes = -(-c.seqs // 128) * 128
    return c


def remote(src, dst, send_sem, recv_sem, axis, peer):
    return pltpu.make_async_remote_copy(
        src_ref=src, dst_ref=dst, send_sem=send_sem, recv_sem=recv_sem,
        device_id={axis: peer}, device_id_type=MESH,
    )


def line(m, sent, mid, came, over, full, sems, over_r):
    z = lax.axis_index("tp")
    half = m // 2
    left = z < half
    depth = jnp.where(left, z, m - 1 - z)
    toward = jnp.where(left, z + 1, z - 1)
    away = lax.rem(jnp.where(left, z - 1, z + 1) + m, m)
    centre = depth == half - 1
    in_s, over_s, full_s, in_r, full_r = sems
    own = sent if half == 1 else mid

    def inward(src, p):
        return remote(src.at[p], came.at[p], in_s, in_r.at[p], "tp", toward)

    def across(p):
        return remote(own.at[p], over.at[p], over_s, over_r.at[p], "tp", toward)

    def outward(p):
        return remote(full.at[p], full.at[p], full_s, full_r.at[p], "tp", away)

    def start(p):
        if half > 1:

            @pl.when(depth == 0)
            def _():
                inward(sent, p).start()

    def relay(p):
        if half > 1:

            @pl.when(depth > 0)
            def _():
                inward(mid, p).wait_recv()
                mid[p] = (sent[p].astype(F32) + came[p].astype(F32)).astype(BF16)

        @pl.when(centre)
        def _():
            across(p).start()

        if half > 2:

            @pl.when((depth > 0) & jnp.logical_not(centre))
            def _():
                inward(mid, p).start()

    def take(p):
        @pl.when(centre)
        def _():
            across(p).wait_recv()
            full[p] = (own[p].astype(F32) + over[p].astype(F32)).astype(BF16)

        if half > 1:

            @pl.when(jnp.logical_not(centre))
            def _():
                outward(p).wait_recv()

            @pl.when(depth > 0)
            def _():
                outward(p).start()

    def end():
        @pl.when(centre)
        def _():
            remote(own, over, over_s, over_r.at[0], "tp", toward).wait_send()

        if half > 1:

            @pl.when(jnp.logical_not(centre))
            def _():
                remote(sent, came, in_s, in_r.at[0], "tp", toward).wait_send()

            @pl.when(depth > 0)
            def _():
                remote(full, full, full_s, full_r.at[0], "tp", away).wait_send()

    return types.SimpleNamespace(start=start, relay=relay, take=take, end=end)


def main_kernel(
    c, counts, resid, wq, wk, wv, wz, wa, wb, wo, speed, bias, scaling, channel, shrink, states,
    tokens, new, *scratch,
):
    s = types.SimpleNamespace(**dict(zip(c.names, scratch)))
    lines = [
        line(
            c.m, s.sent.at[l], s.mid.at[l], s.came.at[l], s.over.at[l], s.full.at[l],
            (s.line_s.at[0], s.line_s.at[1], s.line_s.at[2], s.in_r, s.full_r), s.over_r.at[l],
        )
        for l in range(BLOCKS)
    ]
    n, m, chips, tile = c.n, c.m, c.chips, c.tile
    me = lax.axis_index("dp")
    z = lax.axis_index("tp")
    core = lax.rem(me, 2)
    chip = lax.div(me, 2)
    partner = me + 1 - 2 * core
    others = [lax.rem(me + 2 * d, n) for d in range(1, chips)]
    sources = [lax.rem(me + n - 2 * d, n) for d in range(1, chips)]
    def load(src, dst, sem):
        copy = pltpu.make_async_copy(src, dst, sem)
        copy.start()
        return copy

    all_heads = wa.shape[1]
    ab = 2 * all_heads
    feats = pl.ds(pl.multiple_of(me * c.feat, 128), c.feat)
    early = [
        load(src, dst, s.small_sem.at[i])
        for i, (src, dst) in enumerate(
            [
                (resid, s.resid), (scaling, s.scaling),
                (wa.at[:, :, feats], s.wab.at[:, pl.ds(0, all_heads)]),
                (wb.at[:, :, feats], s.wab.at[:, pl.ds(all_heads, all_heads)]),
            ]
        )
    ]
    wo_loads, state_loads = {}, {}

    def load_weights(l, j):
        for i, w in enumerate((wq, wk, wv, wz)):
            load(w.at[l, :, pl.ds(j * tile, tile)], s.w.at[l, j, :, pl.ds(i * tile, tile)], s.w_sem.at[j])

    def wait_weights(l, j):
        pltpu.make_async_copy(s.w.at[l, j], s.w.at[l, j], s.w_sem.at[j]).wait()

    def load_rest(l):
        state_loads[l] = load(states.at[l], new.at[l], s.state_sem.at[l])
        wo_loads[l] = load(wo.at[l], s.wo.at[l], s.wo_sem.at[l])

    load_weights(0, 0)
    late = [
        load(src, dst, s.small_sem.at[len(early) + i])
        for i, (src, dst) in enumerate(
            [(speed, s.speed), (bias, s.bias), (channel, s.channel), (shrink, s.shrink)]
        )
    ]
    dp_peers = [lax.rem(me + d, n) for d in range(1, n)]
    swaps = [
        remote(s.counts.at[me], s.counts.at[me], s.count_sem.at[0], s.count_sem.at[1], "dp", peer)
        for peer in dp_peers
    ]
    barrier = pltpu.get_barrier_semaphore()

    def greet():
        for axis, peers in (("dp", dp_peers), ("tp", [lax.rem(z + 1, m), lax.rem(z + m - 1, m)])):
            for peer in peers:
                pl.semaphore_signal(barrier, inc=1, device_id={axis: peer}, device_id_type=MESH)

    def fill_counts():
        lane = iota((8, c.lanes), 1) - me * c.own_seqs
        mine = jnp.zeros((8, c.lanes), jnp.int32)
        for i in range(c.own_seqs):
            mine = jnp.where(lane == i, counts[i], mine)
        s.counts[me] = mine

    def swap_counts():
        pl.semaphore_wait(barrier, n + 1)
        for copy in swaps:
            copy.start()

    greet()
    fill_counts()
    swap_counts()

    def constants():
        row = lax.div(iota((tile, tile), 0), c.size)
        col = lax.div(iota((tile, tile), 1), c.size)
        s.blocks[...] = (row == col).astype(BF16)
        for g in range(c.groups):
            r = lax.rem(iota((2 * c.own, tile), 0), c.own_seqs)
            k = g * c.per_tile + lax.div(iota((2 * c.own, tile), 1), c.size)
            s.mask[g] = (r == k).astype(BF16)

    for j in range(1, c.chunks):
        load_weights(0, j)
    constants()
    load_early = lambda: [copy.wait() for copy in early]
    flat = lambda: s.resid[...].reshape(c.rows, c.feat)

    def raw_small():
        load_early()
        wide = flat().astype(F32)
        bent = (wide * s.scaling[...].astype(F32)[:1]).astype(BF16)
        s.bent[...] = bent
        s.raw_small[0] = narrow(bent, s.wab[0]).astype(BF16)
        squares = jnp.sum(wide * wide, axis=1, keepdims=True)
        s.raw_small[1] = jnp.broadcast_to(squares, (c.rows, ab)).astype(BF16)
        raw_swap(-1).start()

    def raw_swap(j):
        x, pair = (s.raw_small, s.raw_pair_small) if j < 0 else (s.raw, s.raw_pair)
        return remote(x.at[1 - core], pair, s.raw_s.at[j + 1], s.first_r.at[j + 1], "dp", partner)

    def raw_first():
        wait_weights(0, 0)
        val = dot(s.bent[...], s.w[0, 0]).astype(BF16)
        s.raw[0] = val[:, : 2 * tile]
        s.raw[1] = val[:, 2 * tile :]
        raw_swap(0).start()

    def wait_counts():
        every = s.counts.at[pl.ds(0, n - 1)]
        swap = remote(every, every, s.count_sem.at[0], s.count_sem.at[1], "dp", partner)
        swap.wait()

    def raw_cross(j):
        x, pair = (s.raw_small, s.raw_pair_small) if j < 0 else (s.raw, s.raw_pair)
        raw_swap(j).wait_recv()
        total = (x[core].astype(F32) + pair[...].astype(F32)).astype(BF16)
        bufs(0, j)[2][...] = dot(s.into[...], total).astype(BF16)
        for d in range(chips - 1):
            second(0, j, d).start()

    raw_small()
    raw_first()
    load_rest(0)
    wait_counts()
    total = s.counts[0]
    for d in range(1, n):
        total = total + s.counts[d]
    row_counts = total.astype(F32)
    row_bf16 = row_counts.astype(BF16)

    def columns(count, seq, slot):
        lanes = iota((count, c.lanes), 1)
        all_counts = jnp.broadcast_to(row_counts[:1], (count, c.lanes))
        start = jnp.sum(jnp.where(lanes < seq, all_counts, 0.0), axis=1, keepdims=True)
        size = jnp.sum(jnp.where(lanes == seq, all_counts, 0.0), axis=1, keepdims=True)
        slot = slot[:, :1].astype(F32)
        return start + slot, slot < size

    def rows_of(seq, slot):
        index = iota(seq.shape, 0)
        start = dot(row_bf16, (index < seq).astype(BF16))[:1]
        size = dot(row_bf16, (index == seq).astype(BF16))[:1]
        slot = slot[:1].astype(F32)
        return start + slot, slot < size

    def pack():
        shape = (c.lanes, c.rows)
        pos, live = rows_of(lax.div(iota(shape, 1), c.slots), lax.rem(iota(shape, 1), c.slots))
        s.into[...] = jnp.where((iota((c.packed, c.rows), 0).astype(F32) == pos) & live, 1.0, 0.0).astype(BF16)

    pack()

    def produce(l, j):
        at = slice((c.pairs - 1) * 2 * c.part, c.feat)
        if l:
            val = s.acc[j] + dot(s.scaled[:, at], s.w[l, j, at])
        else:
            wait_weights(l, j)
            val = dot(s.scaled[...], s.w[l, j])
        val = val.astype(BF16)
        s.x[l, j, 0] = val[:, : 2 * tile]
        s.x[l, j, 1] = val[:, 2 * tile :]
        first(l, j).start()

    def pack_rest():
        h = dot(s.into[...], flat())
        s.h[...] = h
        s.scaled[...] = (h * s.scaling[...].astype(F32)[:1]).astype(BF16)

    def produce_small(l):
        at = slice((c.pairs - 1) * 2 * c.part, c.feat)
        h = s.h[...]
        s.x_small[l, 0] = (s.acc_small[...] + narrow(s.scaled[:, at], s.wab[l, :, at])).astype(BF16)
        squares = jnp.sum(h * h, axis=1, keepdims=True)
        s.x_small[l, 1] = jnp.broadcast_to(squares, (c.packed, ab)).astype(BF16)
        first(l, -1).start()

    def bufs(l, j):
        if j < 0:
            return s.x_small.at[l], s.pair_small.at[l], s.sum_small.at[l], s.far_small.at[l], s.out_small.at[l], s.fin_small.at[l]
        return s.x.at[l, j], s.pair.at[l, j], s.sum.at[l, j], s.far.at[l, j], s.out.at[l, j], s.fin.at[l, j]

    def kind(j):
        return min(j + 1, 1)

    def first(l, j):
        x, pair, *_ = bufs(l, j)
        return remote(x.at[1 - core], pair, s.first_s.at[kind(j)], s.first_r.at[j + 1], "dp", partner)

    def second(l, j, d):
        _, _, own, far, *_ = bufs(l, j)
        there = pl.multiple_of(lax.div(others[d], 2) * c.per_chip, 16)
        return remote(
            own.at[pl.ds(there, c.chip_win)], far.at[d], s.second_s.at[kind(j), d], s.second_r.at[j + 1, d],
            "dp", others[d],
        )

    def third(l, j):
        *_, out, fin = bufs(l, j)
        return remote(out, fin.at[core], s.third_s.at[kind(j)], s.third_r.at[j + 1], "dp", partner)

    def cross(l, j):
        x, pair, own, *_ = bufs(l, j)
        first(l, j).wait_recv()
        own[...] = (x[core].astype(F32) + pair[...].astype(F32)).astype(BF16)
        for d in range(chips - 1):
            second(l, j, d).start()

    def finish(l, j):
        x, pair, own, far, out, fin = bufs(l, j)
        for d in range(chips - 1):
            second(l, j, d).wait_recv()

        def reduced(which):
            at = pl.multiple_of(which * c.own_seqs, 16)
            val = own[pl.ds(pl.multiple_of(chip * c.per_chip + at, 16), c.win), :].astype(F32)
            for d in range(chips - 1):
                val = val + far[d, pl.ds(at, c.win), :].astype(F32)
            return val.astype(BF16)

        out[...] = reduced(1 - core)
        third(l, j).start()
        fin[core] = reduced(core)

    def prepare(l):
        third(l, -1).wait_recv()
        pick = s.pick[...]
        heads = c.heads
        few = dot(pick, s.fin_small[l, 0]).astype(BF16)
        squares = dot(pick, s.fin_small[l, 1])[:, :1]
        factor = lax.rsqrt(squares / (c.feat * n) + EPS)
        s.factor[...] = jnp.broadcast_to(factor, s.factor.shape)
        at = iota((ab, heads), 1) + z * heads
        pa = dot(few, (iota((ab, heads), 0) == at).astype(BF16)) * factor
        pb = dot(few, (iota((ab, heads), 0) == at + all_heads).astype(BF16)) * factor
        arg = pa + s.bias[...][l : l + 1]
        soft = jnp.maximum(arg, 0.0) + jnp.log1p(jnp.exp(-jnp.abs(arg)))
        extra = jnp.concatenate([s.shrink[l, :, t, :] for t in range(c.slots)], axis=0)
        dec = jnp.exp(extra - jnp.exp(s.speed[...][l : l + 1]) * soft)
        dec = jnp.where(s.live[:, :1] > 0.0, dec, 1.0)
        wide = (iota((heads, c.cols), 0) == lax.div(iota((heads, c.cols), 1), c.size)).astype(BF16)
        both = jnp.concatenate([dec, jax.nn.sigmoid(pb)], axis=0)
        high = both.astype(BF16)
        low = (both - high.astype(F32)).astype(BF16)
        spread = dot(jnp.concatenate([high, low], axis=0), wide)
        s.dec[...] = spread[: c.own] + spread[2 * c.own : 3 * c.own]
        s.beta[...] = spread[c.own : 2 * c.own] + spread[3 * c.own :]

    def recur(l, j):
        at = slice(j * tile, (j + 1) * tile)
        third(l, j).wait_recv()
        pick = s.pick[...]
        factor = s.factor[:, :1]
        qk = dot(pick, s.fin[l, j, 0]) * factor
        vz = dot(pick, s.fin[l, j, 1]) * factor
        qk = qk * jax.nn.sigmoid(qk)
        vz = vz * jax.nn.sigmoid(vz)
        q, k = qk[:, :tile], qk[:, tile:]
        v, zed = vz[:, :tile], vz[:, tile:]
        both = jnp.concatenate([k, q], axis=0)
        low = iota((2 * c.own, 128), 1) < c.size
        copies = []
        for i in range(tile // 128):
            here = both[:, i * 128 : (i + 1) * 128]
            turned = pltpu.roll(here, c.size, 1)
            copies += [jnp.where(low, here, turned), jnp.where(low, turned, here)]
        lhs = []
        for one in copies:
            wide = jnp.concatenate([one.astype(BF16)] * (tile // 128), axis=1)
            lhs.append(jnp.concatenate([wide * s.mask[g] for g in range(c.groups)], axis=1))
        read = dot(jnp.concatenate(lhs, axis=0), s.states16[l, :, at])
        step = lambda x, t: x[t * c.own_seqs : (t + 1) * c.own_seqs]
        names, prods = [], []
        for t in range(c.slots):
            names.append(("n", t, t))
            prods.append(step(q, t) * step(q, t))
            for i in range(t + 1):
                names.append(("q", i, t))
                prods.append(step(k, i) * step(q, t))
                names.append(("k", i, t))
                prods.append(step(k, i) * step(k, t))
        pairs = dot(jnp.concatenate(prods, axis=0).astype(BF16), s.blocks[...])
        pairs = {name: step(pairs, i) for i, name in enumerate(names)}
        nk = [lax.rsqrt(pairs["k", t, t] + EPS) for t in range(c.slots)]
        nq = [lax.rsqrt(pairs["n", t, t] + EPS) * c.size ** (-0.5) for t in range(c.slots)]
        s.k[l, :, at] = (k * jnp.concatenate(nk, axis=0)).astype(BF16)
        lane_head = lax.div(iota((2 * c.own, tile), 1), c.size)
        reads = read[: 2 * c.own]
        for h in range(1, c.per_tile):
            reads = jnp.where(lane_head == h, read[2 * c.own * h : 2 * c.own * (h + 1)], reads)
        rk = reads[: c.own]
        rq = reads[c.own :]
        dec = s.dec[:, at]
        beta = s.beta[:, at]
        fresh, outs = [], []
        whole = None
        for t in range(c.slots):
            g = step(dec, t)
            whole = g if whole is None else whole * g
            fresh = [(u * g) for u in fresh]
            guess = whole * step(rk, t)
            for i in range(t):
                guess = guess + pairs["k", i, t] * nk[i] * fresh[i]
            fresh.append(step(beta, t) * (step(v, t) - guess * nk[t]))
            o = whole * step(rq, t)
            for i in range(t + 1):
                o = o + pairs["q", i, t] * nk[i] * fresh[i]
            outs.append(o * nq[t])
        s.u[l, :, at] = jnp.concatenate(fresh, axis=0).astype(BF16)
        s.decay[l, :, at] = whole
        o = jnp.concatenate(outs, axis=0)
        total = dot((o * o).astype(BF16), s.blocks[...])
        o = o * lax.rsqrt(total / c.size + EPS) * s.gain[l, :1] * zed
        s.y[l, me, j] = dot(s.place[...], o.astype(BF16)).astype(BF16)
        for d in range(chips - 1):
            y_far(l, j, d).start()
        y_near(l, j, 0).start()

    def y_far(l, j, d):
        here = s.y.at[l, me, j]
        return remote(here, here, s.yf_s.at[d], s.yf_r.at[j, d], "dp", others[d])

    def y_near(l, j, d):
        source = me if d == 0 else sources[d - 1]
        here = s.y.at[l, source, j]
        return remote(here, here, s.yn_s.at[d], s.yn_r.at[0], "dp", partner)

    def forward(l, j):
        for d in range(chips - 1):
            y_far(l, j, d).wait_recv()
            y_near(l, j, d + 1).start()

    def near_all(l):
        every = s.y.at[l, pl.ds(0, chips)]
        remote(every, every, s.yn_s.at[0], s.yn_r.at[0], "dp", partner).wait_recv()

    def sent_all(l):
        if l:
            first(l, -1).wait_send()
        else:
            for j in (-1, 0):
                raw_swap(j).wait_send()
        if l or c.chunks > 1:
            done = s.pair.at[l] if l else s.pair.at[l, pl.ds(1, c.chunks - 1)]
            remote(done, done, s.first_s.at[1], s.first_r.at[0], "dp", partner).wait_send()
        for d in range(chips - 1):
            second(l, -1, d).wait_send()
            done = s.far.at[l, :, d]
            remote(done, done, s.second_s.at[1, d], s.second_r.at[0, d], "dp", others[d]).wait_send()
            done = s.y.at[l, me]
            remote(done, done, s.yf_s.at[d], s.yf_r.at[0, d], "dp", others[d]).wait_send()
        third(l, -1).wait_send()
        done = s.out.at[l]
        remote(done, done, s.third_s.at[1], s.third_r.at[0], "dp", partner).wait_send()
        for d in range(chips):
            done = s.y.at[l, me]
            remote(done, done, s.yn_s.at[d], s.yn_r.at[0], "dp", partner).wait_send()

    def gather(l, j):
        at = slice(j * tile, (j + 1) * tile)
        s.gated[:, at] = jnp.zeros((c.packed, tile), BF16)
        for d in range(n):
            here = slice(d * c.own_seqs, d * c.own_seqs + c.win)
            s.gated[here, at] = s.gated[here, at] + s.y[l, d, j]

    def mix_mul(l, run):
        per = c.parts // 2
        at = slice(run * per * c.part, (run + 1) * per * c.part)
        val = dot(s.gated[...], s.wo[l, :, at]).astype(BF16)
        for i in range(per):
            s.sent[l, run * per + i] = val[:, i * c.part : (i + 1) * c.part]
        for i in range(per):
            lines[l].start(run * per + i)

    def mix_out(l, p):
        lines[l].relay(p)

    def mix_in(l, p):
        lines[l].take(p)
        at = slice(p * c.part, (p + 1) * c.part)
        mixed = (s.h[:, at] + s.full[l, p].astype(F32)).astype(BF16)
        s.scaled[:, at] = mixed
        if l + 1 < BLOCKS:
            mixed = mixed.astype(F32)
            s.h[:, at] = mixed
            s.scaled[:, at] = (mixed * s.scaling[...].astype(F32)[l + 1 : l + 2, at]).astype(BF16)

    def place_tokens(p):
        at = slice((p - 1) * c.part, (p + 1) * c.part)
        back = dot(s.hot[...], s.scaled[:, at])
        kept = s.resid[:, :, at].reshape(c.rows, 2 * c.part).astype(F32)
        mixed = jnp.where(s.alive[:, :1] > 0.0, back, kept).astype(BF16)
        tokens[:, :, at] = mixed.reshape(c.seqs, c.slots, 2 * c.part)

    def setup():
        r = iota((c.own, c.lanes), 0)
        pos, live = columns(c.own, lax.rem(r, c.own_seqs) + me * c.own_seqs, lax.div(r, c.own_seqs))
        offset = (iota((c.own, c.win), 1) + me * c.own_seqs).astype(F32)
        s.pick[...] = jnp.where((offset == pos) & live, 1.0, 0.0).astype(BF16)
        s.live[...] = jnp.broadcast_to(jnp.where(live, 1.0, 0.0), s.live.shape)
        shape = (c.lanes, c.own)
        pos, live = rows_of(
            lax.rem(iota(shape, 1), c.own_seqs) + me * c.own_seqs, lax.div(iota(shape, 1), c.own_seqs)
        )
        offset = (iota((c.win, c.own), 0) + me * c.own_seqs).astype(F32)
        s.place[...] = jnp.where((offset == pos) & live, 1.0, 0.0).astype(BF16)
        r = iota((c.rows, c.lanes), 0)
        pos, live = columns(c.rows, lax.div(r, c.slots), lax.rem(r, c.slots))
        offset = iota((c.rows, c.packed), 1).astype(F32)
        s.alive[...] = jnp.broadcast_to(jnp.where(live, 1.0, 0.0), s.alive.shape)
        s.hot[...] = jnp.where((offset == pos) & live, 1.0, 0.0).astype(BF16)
        fold = (iota((c.size, tile), 0) == lax.rem(iota((c.size, tile), 1), c.size)).astype(BF16)
        for l in range(BLOCKS):
            channels = jnp.broadcast_to(s.channel[...].astype(F32)[l : l + 1], (8, c.size)).astype(BF16)
            s.gain[l] = dot(channels, fold)

    def write_states(l, j):
        at = slice(j * tile, (j + 1) * tile)
        shape = (c.per_tile * c.own, tile)
        same = (lax.div(iota(shape, 0), c.own) == lax.div(iota(shape, 1), c.size)).astype(BF16)
        fold = (iota((c.size, tile), 0) == lax.rem(iota((c.size, tile), 1), c.size)).astype(BF16)
        keys = lax.dot_general(
            fold, tiles(s.k[l, :, at], c.per_tile) * same, (((1,), (1,)), ((), ())), preferred_element_type=F32
        ).astype(BF16)
        fresh = tiles(s.u[l, :, at], c.per_tile) * same
        owner = lax.rem(iota((c.size, c.per_tile * c.own), 1), c.own_seqs)
        batch = 4
        for first_seq in range(0, c.own_seqs, batch):
            lhs = jnp.concatenate(
                [keys * (owner == first_seq + i).astype(BF16) for i in range(batch)], axis=0
            )
            added = dot(lhs, fresh)
            for i in range(batch):
                seq = first_seq + i
                new[l, seq, :, at] = (
                    new[l, seq, :, at] * s.decay[l, seq : seq + 1, at] + added[i * c.size : (i + 1) * c.size]
                )

    def round_states(l):
        state_loads[l].wait()
        for i in range(c.own_seqs):
            s.states16[l, i * c.size : (i + 1) * c.size] = new[l, i].astype(BF16)

    for l in range(BLOCKS):
        if l:
            for j in range(c.chunks):
                wait_weights(l, j)
            for p in range(c.parts):
                mix_in(l - 1, p)
                if p % 2 and p + 1 < c.parts:
                    at = slice((p - 1) * c.part, (p + 1) * c.part)
                    piece = s.scaled[:, at]
                    for j in range(c.chunks):
                        val = dot(piece, s.w[l, j, at])
                        s.acc[j] = val if p == 1 else s.acc[j] + val
                    val = narrow(piece, s.wab[l, :, at])
                    s.acc_small[...] = val if p == 1 else s.acc_small[...] + val
        if l:
            produce_small(l)
            produce(l, 0)
        else:
            raw_cross(-1)
            raw_cross(0)
            pack_rest()
        for j in range(1, c.chunks):
            produce(l, j)
            if l:
                cross(l, j - 2)
            elif j > 1:
                cross(l, j - 1)
        if l:
            cross(l, c.chunks - 2)
        if l or c.chunks > 1:
            cross(l, c.chunks - 1)
        if l == 0:
            for j in range(c.chunks):
                load_weights(1, j)
            load_rest(1)
            for copy in late:
                copy.wait()
            setup()
            round_states(0)
        finish(l, -1)
        prepare(l)
        finish(l, 0)
        for j in range(1, c.chunks):
            finish(l, j)
            recur(l, j - 1)
        recur(l, c.chunks - 1)
        for j in range(c.chunks):
            forward(l, j)
            if j >= 1:
                write_states(l, j - 1)
        wo_loads[l].wait()
        near_all(l)
        for j in range(c.chunks):
            gather(l, j)
        mix_mul(l, 0)
        mix_mul(l, 1)
        write_states(l, c.chunks - 1)
        if l == 0:
            round_states(1)
        if l:
            lines[l - 1].end()
        for p in range(c.parts):
            mix_out(l, p)
        sent_all(l)
    for p in range(c.parts):
        mix_in(BLOCKS - 1, p)
        if p % 2:
            place_tokens(p)
    lines[BLOCKS - 1].end()


def run_main(c, args):
    ab = 2 * args[6].shape[1]
    half = 2 * c.tile
    chips, n = c.chips, c.n
    dma = lambda *shape: pltpu.SemaphoreType.DMA(shape)
    buf = lambda *shape: pltpu.VMEM(shape, BF16)
    wide = lambda *shape: pltpu.VMEM(shape, F32)
    every = 1 + c.chunks
    scratch = dict(
        resid=buf(c.seqs, c.slots, c.feat),
        k=buf(BLOCKS, c.own, c.cols),
        u=buf(BLOCKS, c.own, c.cols),
        decay=wide(BLOCKS, c.own_seqs, c.cols),
        scaling=buf(BLOCKS, c.feat),
        wab=buf(BLOCKS, ab, c.feat),
        speed=wide(BLOCKS, c.heads),
        bias=wide(BLOCKS, c.heads),
        channel=buf(BLOCKS, c.size),
        shrink=wide(BLOCKS, c.own_seqs, c.slots, c.heads),
        w=buf(BLOCKS, c.chunks, c.feat, 4 * c.tile),
        raw=buf(2, c.rows, half),
        raw_small=buf(2, c.rows, ab),
        raw_pair=buf(c.rows, half),
        raw_pair_small=buf(c.rows, ab),
        hot=buf(c.rows, c.packed),
        alive=wide(c.rows, 128),
        **{name: buf(BLOCKS, c.parts, c.packed, c.part) for name in ("sent", "mid", "came", "over", "full")},
        bent=buf(c.rows, c.feat),
        into=buf(c.packed, c.rows),
        wo=buf(BLOCKS, c.cols, c.feat),
        states16=buf(BLOCKS, c.own_seqs * c.size, c.cols),
        counts=pltpu.VMEM((n, 8, c.lanes), jnp.int32),
        blocks=buf(c.tile, c.tile),
        mask=buf(c.groups, 2 * c.own, c.tile),
        gain=wide(BLOCKS, 8, c.tile),
        pick=buf(c.own, c.win),
        place=buf(c.win, c.own),
        live=wide(c.own, 128),
        factor=wide(c.own, 128),
        dec=wide(c.own, c.cols),
        beta=wide(c.own, c.cols),
        h=wide(c.packed, c.feat),
        scaled=buf(c.packed, c.feat),
        acc=wide(c.chunks, c.packed, 4 * c.tile),
        acc_small=wide(c.packed, ab),
        x=buf(BLOCKS, c.chunks, 2, c.packed, half),
        pair=buf(BLOCKS, c.chunks, c.packed, half),
        sum=buf(BLOCKS, c.chunks, c.packed, half),
        far=buf(BLOCKS, c.chunks, chips - 1, c.chip_win, half),
        out=buf(BLOCKS, c.chunks, c.win, half),
        fin=buf(BLOCKS, c.chunks, 2, c.win, half),
        x_small=buf(BLOCKS, 2, c.packed, ab),
        pair_small=buf(BLOCKS, c.packed, ab),
        sum_small=buf(BLOCKS, c.packed, ab),
        far_small=buf(BLOCKS, chips - 1, c.chip_win, ab),
        out_small=buf(BLOCKS, c.win, ab),
        fin_small=buf(BLOCKS, 2, c.win, ab),
        y=buf(BLOCKS, n, c.chunks, c.win, c.tile),
        gated=buf(c.packed, c.cols),
        small_sem=dma(8),
        w_sem=dma(c.chunks),
        wo_sem=dma(BLOCKS),
        state_sem=dma(BLOCKS),
        count_sem=dma(2),
        raw_s=dma(2),
        first_s=dma(2),
        first_r=dma(every),
        second_s=dma(2, chips - 1),
        second_r=dma(every, chips - 1),
        third_s=dma(2),
        third_r=dma(every),
        yf_s=dma(chips - 1),
        yf_r=dma(c.chunks, chips - 1),
        yn_s=dma(chips),
        yn_r=dma(1),
        line_s=dma(3),
        in_r=dma(c.parts),
        full_r=dma(c.parts),
        over_r=dma(BLOCKS, c.parts),
    )
    c.names = list(scratch)
    return pl.pallas_call(
        functools.partial(main_kernel, c),
        out_shape=[
            pltpu.VMEM(args[1].shape, BF16),
            pltpu.VMEM(args[-1].shape, F32),
        ],
        in_specs=[SMEM] + [HBM] * 14,
        out_specs=[VMEM] * 2,
        scratch_shapes=list(scratch.values()),
        compiler_params=pltpu.CompilerParams(
            collective_id=1, has_side_effects=True, vmem_limit_bytes=46 * 1024 * 1024
        ),
        name="blocks",
    )(*[args[0]] + [pltpu.with_memory_space_constraint(x, pltpu.HBM) for x in args[1:]])


def store_kernel(pieces, tokens, new, tokens_out, new_out, sem):
    copies = [pltpu.make_async_copy(tokens, tokens_out, sem.at[pieces])]
    size = new.shape[1] * new.shape[0] // pieces
    for i in range(pieces):
        l, at = divmod(i * size, new.shape[1])
        at = pl.ds(at, size)
        copies.append(pltpu.make_async_copy(new.at[l, at], new_out.at[l, at], sem.at[i]))
    for copy in copies:
        copy.start()
    for copy in copies:
        copy.wait()


def store(tokens, new):
    pieces = 8
    return pl.pallas_call(
        functools.partial(store_kernel, pieces),
        out_shape=[jax.ShapeDtypeStruct(a.shape, a.dtype) for a in (tokens, new)],
        in_specs=[VMEM] * 2,
        out_specs=[HBM] * 2,
        scratch_shapes=[pltpu.SemaphoreType.DMA((pieces + 1,))],
        compiler_params=pltpu.CompilerParams(vmem_limit_bytes=1024 * 1024),
        name="store",
    )(tokens, new)


def body(
    n, m, resid, counts, wq, wk, wv, wz, wa, wb, wo, speed, bias, scaling, channel, shrink, states,
):
    c = sizes(n, m, resid, counts, wq, speed)
    turned = [jnp.swapaxes(w, 1, 2) for w in (wa, wb)]
    tokens, new = run_main(
        c, (counts, resid, wq, wk, wv, wz, *turned, wo, speed, bias, scaling, channel, shrink, states)
    )
    return store(tokens, new)


def solution(mesh):
    in_specs = (
        P("grp", None, "dp"),
        P(("grp", "dp")),
        P(None, "dp", "tp"),
        P(None, "dp", "tp"),
        P(None, "dp", "tp"),
        P(None, "dp", "tp"),
        P(),
        P(),
        P(None, "tp", "dp"),
        P(None, "tp"),
        P(None, "tp"),
        P(None, "dp"),
        P(),
        P(None, ("grp", "dp"), None, "tp"),
        P(None, ("grp", "dp"), None, "tp"),
    )
    out_specs = (P("grp", None, "dp"), P(None, ("grp", "dp"), None, "tp"))
    run = functools.partial(body, mesh.shape["dp"], mesh.shape["tp"])
    return jax.shard_map(run, mesh=mesh, in_specs=in_specs, out_specs=out_specs, check_vma=False)
```

time: 80.1 us -> 70.1 us (0.88)
  Pallas kernels: 74.4 us -> 69.2 us
  local copies, waits for them, and re-layouts: 4.84 us -> 0 us
    pallas_call x1, Pallas kernels: 74.4 us -> 65.6 us  [run_main(): pl.pallas_call(functools.partial(main_kernel, c), out_shape=[pltpu.VMEM(a...]
    unnamed x4 -> x0, local copies, waits for them, and re-layouts: 4.84 us -> none
    pallas_call x0 -> x1, Pallas kernels: none -> 3.55 us  [store(): pl.pallas_call(functools.partial(store_kernel, pieces), out_shape=[jax.Sh...]
where the time goes in v3:
time: 70.1 us; the launch traced here: 70 us
  Pallas kernels  69.2 us (99%)
  between operations  0.8 us (1%)
    pallas_call x1, Pallas kernels, run_main(): pl.pallas_call(functools.partial(main_kernel, c), out_shape=[pltpu.VMEM(a...  65.6 us
    pallas_call x1, Pallas kernels, store(): pl.pallas_call(functools.partial(store_kernel, pieces), out_shape=[jax.Sh...  3.55 us

profile of v3, /device:TPU:0, one launch (start us, length us, event | category | flops | bytes accessed | tf_op | source)
XLA Modules:
  0.0 70.0 jit_solution(10996807557706281161)
XLA Ops:
  0.6 65.6 %blocks.1 = (bf16[64,4,1024]{2,1,0:T(4,128)(2,1)S(1)}, f32[2,16,64,1024]{3,2,1,0:T(8,128)S(1)}) custom-call(s32[16]{0:T(128)} %counts.1, bf16[64,4,1024]{2,1,0:T(4,128)(2,1)} %resid.1, bf16[2,1024,1024]{2,1,0:T(8,128)(2,1)} %wq.1, bf16[2,1024,1024]{2,1,0:T(8,128)(2,1)} %wk.1, bf16[2,1024,1024]{2,1,0:T(8,128)(2,1)} %wv.1, bf16[2,1024,1024]{2,1,0:T(8,128)(2,1)} %wz.1, ...), custom_call_target="tpu_custom_call" | custom-call | tf_op jit(solution)/shard_map/blocks/pallas_call | solution.py:758
  66.3 3.5 %store.1 = (bf16[64,4,1024]{2,1,0:T(4,128)(2,1)}, f32[2,16,64,1024]{3,2,1,0:T(8,128)}) custom-call(bf16[64,4,1024]{2,1,0:T(4,128)(2,1)S(1)} %get-tuple-element.4.tokens, f32[2,16,64,1024]{3,2,1,0:T(8,128)S(1)} %get-tuple-element.5.new), custom_call_target="tpu_custom_call" | custom-call | tf_op jit(solution)/shard_map/store/pallas_call | solution.py:789

commit v4 on v3

--- a/solution.py
+++ b/solution.py
@@ -15,7 +15,6 @@
 MESH = pl.DeviceIdType.MESH
 VMEM = pl.BlockSpec(memory_space=pltpu.VMEM)
 HBM = pl.BlockSpec(memory_space=pltpu.HBM)
-SMEM = pl.BlockSpec(memory_space=pltpu.SMEM)
 
 
 def iota(shape, dim):
@@ -54,6 +53,7 @@
     c.groups = c.own_seqs // c.per_tile
     c.parts = 8
     c.pairs = c.parts // 2
+    c.direct = 5 if m == 4 else 0
     c.part = c.feat // c.parts
     c.lanes = -(-c.seqs // 128) * 128
     return c
@@ -66,7 +66,7 @@
     )
 
 
-def line(m, sent, mid, came, over, full, sems, over_r):
+def line(m, direct, sent, mid, came, over, full, sems, over_r, early_r):
     z = lax.axis_index("tp")
     half = m // 2
     left = z < half
@@ -74,8 +74,10 @@
     toward = jnp.where(left, z + 1, z - 1)
     away = lax.rem(jnp.where(left, z - 1, z + 1) + m, m)
     centre = depth == half - 1
-    in_s, over_s, full_s, in_r, full_r = sems
+    in_s, over_s, full_s, jump_s, in_r, full_r = sems
     own = sent if half == 1 else mid
+    parts = sent.shape[0]
+    straight = parts - direct
 
     def inward(src, p):
         return remote(src.at[p], came.at[p], in_s, in_r.at[p], "tp", toward)
@@ -86,7 +88,20 @@
     def outward(p):
         return remote(full.at[p], full.at[p], full_s, full_r.at[p], "tp", away)
 
+    def early(p):
+        return remote(sent.at[p], came.at[p], in_s, early_r.at[p - straight], "tp", away)
+
+    def jump(p):
+        far = 2 * toward - z
+        return remote(own.at[p], over.at[p], jump_s, over_r.at[p], "tp", far)
+
     def start(p):
+        if p >= straight:
+
+            @pl.when(centre)
+            def _():
+                early(p).start()
+
         if half > 1:
 
             @pl.when(depth == 0)
@@ -103,6 +118,8 @@
 
         @pl.when(centre)
         def _():
+            if p >= straight:
+                jump(p).start()
             across(p).start()
 
         if half > 2:
@@ -117,7 +134,16 @@
             across(p).wait_recv()
             full[p] = (own[p].astype(F32) + over[p].astype(F32)).astype(BF16)
 
-        if half > 1:
+        if p >= straight:
+
+            @pl.when(depth == 0)
+            def _():
+                early(p).wait_recv()
+                mid[p] = (sent[p].astype(F32) + came[p].astype(F32)).astype(BF16)
+                jump(p).wait_recv()
+                full[p] = (mid[p].astype(F32) + over[p].astype(F32)).astype(BF16)
+
+        elif half > 1:
 
             @pl.when(jnp.logical_not(centre))
             def _():
@@ -131,6 +157,10 @@
         @pl.when(centre)
         def _():
             remote(own, over, over_s, over_r.at[0], "tp", toward).wait_send()
+            if direct:
+                some = sent.at[pl.ds(0, direct)]
+                remote(some, some, in_s, in_r.at[0], "tp", away).wait_send()
+                remote(some, some, jump_s, in_r.at[0], "tp", away).wait_send()
 
         if half > 1:
 
@@ -140,7 +170,8 @@
 
             @pl.when(depth > 0)
             def _():
-                remote(full, full, full_s, full_r.at[0], "tp", away).wait_send()
+                some = full.at[pl.ds(0, straight)]
+                remote(some, some, full_s, full_r.at[0], "tp", away).wait_send()
 
     return types.SimpleNamespace(start=start, relay=relay, take=take, end=end)
 
@@ -152,8 +183,9 @@
     s = types.SimpleNamespace(**dict(zip(c.names, scratch)))
     lines = [
         line(
-            c.m, s.sent.at[l], s.mid.at[l], s.came.at[l], s.over.at[l], s.full.at[l],
-            (s.line_s.at[0], s.line_s.at[1], s.line_s.at[2], s.in_r, s.full_r), s.over_r.at[l],
+            c.m, c.direct, s.sent.at[l], s.mid.at[l], s.came.at[l], s.over.at[l], s.full.at[l],
+            (s.line_s.at[0], s.line_s.at[1], s.line_s.at[2], s.line_s.at[3], s.in_r, s.full_r),
+            s.over_r.at[l], s.early_r.at[l],
         )
         for l in range(BLOCKS)
     ]
@@ -164,7 +196,7 @@
     chip = lax.div(me, 2)
     partner = me + 1 - 2 * core
     others = [lax.rem(me + 2 * d, n) for d in range(1, chips)]
-    sources = [lax.rem(me + n - 2 * d, n) for d in range(1, chips)]
+    across_core = [lax.rem(partner + 2 * d, n) for d in range(1, chips)]
     def load(src, dst, sem):
         copy = pltpu.make_async_copy(src, dst, sem)
         copy.start()
@@ -208,10 +240,11 @@
         remote(s.counts.at[me], s.counts.at[me], s.count_sem.at[0], s.count_sem.at[1], "dp", peer)
         for peer in dp_peers
     ]
+    tp_peers = [lax.rem(z + d, m) for d in ((1, 2, 3) if c.direct else (1, m - 1))]
     barrier = pltpu.get_barrier_semaphore()
 
     def greet():
-        for axis, peers in (("dp", dp_peers), ("tp", [lax.rem(z + 1, m), lax.rem(z + m - 1, m)])):
+        for axis, peers in (("dp", dp_peers), ("tp", tp_peers)):
             for peer in peers:
                 pl.semaphore_signal(barrier, inc=1, device_id={axis: peer}, device_id_type=MESH)
 
@@ -219,15 +252,17 @@
         lane = iota((8, c.lanes), 1) - me * c.own_seqs
         mine = jnp.zeros((8, c.lanes), jnp.int32)
         for i in range(c.own_seqs):
-            mine = jnp.where(lane == i, counts[i], mine)
+            mine = jnp.where(lane == i, s.own_counts[i], mine)
         s.counts[me] = mine
 
     def swap_counts():
-        pl.semaphore_wait(barrier, n + 1)
+        pl.semaphore_wait(barrier, len(dp_peers) + len(tp_peers))
         for copy in swaps:
             copy.start()
 
+    own_counts = load(counts, s.own_counts, s.small_sem.at[8])
     greet()
+    own_counts.wait()
     fill_counts()
     swap_counts()
 
@@ -474,27 +509,14 @@
         total = dot((o * o).astype(BF16), s.blocks[...])
         o = o * lax.rsqrt(total / c.size + EPS) * s.gain[l, :1] * zed
         s.y[l, me, j] = dot(s.place[...], o.astype(BF16)).astype(BF16)
-        for d in range(chips - 1):
-            y_far(l, j, d).start()
-        y_near(l, j, 0).start()
-
-    def y_far(l, j, d):
-        here = s.y.at[l, me, j]
-        return remote(here, here, s.yf_s.at[d], s.yf_r.at[j, d], "dp", others[d])
-
-    def y_near(l, j, d):
-        source = me if d == 0 else sources[d - 1]
-        here = s.y.at[l, source, j]
-        return remote(here, here, s.yn_s.at[d], s.yn_r.at[0], "dp", partner)
-
-    def forward(l, j):
-        for d in range(chips - 1):
-            y_far(l, j, d).wait_recv()
-            y_near(l, j, d + 1).start()
-
-    def near_all(l):
-        every = s.y.at[l, pl.ds(0, chips)]
-        remote(every, every, s.yn_s.at[0], s.yn_r.at[0], "dp", partner).wait_recv()
+        for peer in others + across_core + [partner]:
+            here = s.y.at[l, me, j]
+            remote(here, here, s.y_s.at[0], s.y_r.at[int(j + 1 == c.chunks)], "dp", peer).start()
+
+    def wait_y(l, last):
+        chunks = c.chunks - 1 if last else pl.ds(0, c.chunks - 1)
+        every = s.y.at[l, pl.ds(0, n - 1), chunks]
+        remote(every, every, s.y_s.at[0], s.y_r.at[int(last)], "dp", partner).wait_recv()
 
     def sent_all(l):
         if l:
@@ -509,14 +531,11 @@
             second(l, -1, d).wait_send()
             done = s.far.at[l, :, d]
             remote(done, done, s.second_s.at[1, d], s.second_r.at[0, d], "dp", others[d]).wait_send()
-            done = s.y.at[l, me]
-            remote(done, done, s.yf_s.at[d], s.yf_r.at[0, d], "dp", others[d]).wait_send()
         third(l, -1).wait_send()
         done = s.out.at[l]
         remote(done, done, s.third_s.at[1], s.third_r.at[0], "dp", partner).wait_send()
-        for d in range(chips):
-            done = s.y.at[l, me]
-            remote(done, done, s.yn_s.at[d], s.yn_r.at[0], "dp", partner).wait_send()
+        done = s.y.at[l, pl.ds(0, n - 1)]
+        remote(done, done, s.y_s.at[0], s.y_r.at[0], "dp", partner).wait_send()
 
     def gather(l, j):
         at = slice(j * tile, (j + 1) * tile)
@@ -525,10 +544,18 @@
             here = slice(d * c.own_seqs, d * c.own_seqs + c.win)
             s.gated[here, at] = s.gated[here, at] + s.y[l, d, j]
 
+    def mix_some(l):
+        before = slice(0, (c.chunks - 1) * tile)
+        s.mixed[...] = dot(s.gated[:, before], s.wo[l, before])
+
     def mix_mul(l, run):
         per = c.parts // 2
         at = slice(run * per * c.part, (run + 1) * per * c.part)
-        val = dot(s.gated[...], s.wo[l, :, at]).astype(BF16)
+        after = slice((c.chunks - 1) * tile, c.cols)
+        val = dot(s.gated[:, after], s.wo[l, after, at])
+        if c.chunks > 1:
+            val = val + s.mixed[:, at]
+        val = val.astype(BF16)
         for i in range(per):
             s.sent[l, run * per + i] = val[:, i * c.part : (i + 1) * c.part]
         for i in range(per):
@@ -643,20 +670,22 @@
             setup()
             round_states(0)
         finish(l, -1)
+        finish(l, 0)
         prepare(l)
-        finish(l, 0)
         for j in range(1, c.chunks):
             finish(l, j)
             recur(l, j - 1)
         recur(l, c.chunks - 1)
-        for j in range(c.chunks):
-            forward(l, j)
-            if j >= 1:
-                write_states(l, j - 1)
+        for j in range(c.chunks - 1):
+            write_states(l, j)
         wo_loads[l].wait()
-        near_all(l)
-        for j in range(c.chunks):
-            gather(l, j)
+        if c.chunks > 1:
+            wait_y(l, False)
+            for j in range(c.chunks - 1):
+                gather(l, j)
+            mix_some(l)
+        wait_y(l, True)
+        gather(l, c.chunks - 1)
         mix_mul(l, 0)
         mix_mul(l, 1)
         write_states(l, c.chunks - 1)
@@ -733,7 +762,9 @@
         fin_small=buf(BLOCKS, 2, c.win, ab),
         y=buf(BLOCKS, n, c.chunks, c.win, c.tile),
         gated=buf(c.packed, c.cols),
-        small_sem=dma(8),
+        mixed=wide(c.packed, c.feat),
+        own_counts=pltpu.SMEM((c.own_seqs,), jnp.int32),
+        small_sem=dma(9),
         w_sem=dma(c.chunks),
         wo_sem=dma(BLOCKS),
         state_sem=dma(BLOCKS),
@@ -745,11 +776,10 @@
         second_r=dma(every, chips - 1),
         third_s=dma(2),
         third_r=dma(every),
-        yf_s=dma(chips - 1),
-        yf_r=dma(c.chunks, chips - 1),
-        yn_s=dma(chips),
-        yn_r=dma(1),
-        line_s=dma(3),
+        y_s=dma(1),
+        y_r=dma(2),
+        line_s=dma(4),
+        early_r=dma(BLOCKS, max(c.direct, 1)),
         in_r=dma(c.parts),
         full_r=dma(c.parts),
         over_r=dma(BLOCKS, c.parts),
@@ -761,14 +791,14 @@
             pltpu.VMEM(args[1].shape, BF16),
             pltpu.VMEM(args[-1].shape, F32),
         ],
-        in_specs=[SMEM] + [HBM] * 14,
+        in_specs=[HBM] * 15,
         out_specs=[VMEM] * 2,
         scratch_shapes=list(scratch.values()),
         compiler_params=pltpu.CompilerParams(
             collective_id=1, has_side_effects=True, vmem_limit_bytes=46 * 1024 * 1024
         ),
         name="blocks",
-    )(*[args[0]] + [pltpu.with_memory_space_constraint(x, pltpu.HBM) for x in args[1:]])
+    )(*[pltpu.with_memory_space_constraint(x, pltpu.HBM) for x in args])
 
 
 def store_kernel(pieces, tokens, new, tokens_out, new_out, sem):

time: 70.1 us -> 65.8 us (0.939)
  Pallas kernels: 69.2 us -> 64.9 us
    pallas_call x1, Pallas kernels: 65.6 us -> 61.3 us  [run_main(): pl.pallas_call(functools.partial(main_kernel, c), out_shape=[pltpu.VMEM(a...]
where the time goes in v4:
time: 65.8 us; the launch traced here: 65.7 us
  Pallas kernels  64.9 us (99%)
  between operations  0.8 us (1%)
    pallas_call x1, Pallas kernels, run_main(): pl.pallas_call(functools.partial(main_kernel, c), out_shape=[pltpu.VMEM(a...  61.3 us
    pallas_call x1, Pallas kernels, store(): pl.pallas_call(functools.partial(store_kernel, pieces), out_shape=[jax.Sh...  3.55 us

profile of v4, /device:TPU:0, one launch (start us, length us, event | category | flops | bytes accessed | tf_op | source)
XLA Modules:
  0.0 65.7 jit_solution(5584601942337417189)
XLA Ops:
  0.6 61.3 %blocks.1 = (bf16[64,4,1024]{2,1,0:T(4,128)(2,1)S(1)}, f32[2,16,64,1024]{3,2,1,0:T(8,128)S(1)}) custom-call(s32[16]{0:T(128)} %counts.1, bf16[64,4,1024]{2,1,0:T(4,128)(2,1)} %resid.1, bf16[2,1024,1024]{2,1,0:T(8,128)(2,1)} %wq.1, bf16[2,1024,1024]{2,1,0:T(8,128)(2,1)} %wk.1, bf16[2,1024,1024]{2,1,0:T(8,128)(2,1)} %wv.1, bf16[2,1024,1024]{2,1,0:T(8,128)(2,1)} %wz.1, ...), custom_call_target="tpu_custom_call" | custom-call | tf_op jit(solution)/shard_map/blocks/pallas_call | solution.py:788
  62.0 3.5 %store.1 = (bf16[64,4,1024]{2,1,0:T(4,128)(2,1)}, f32[2,16,64,1024]{3,2,1,0:T(8,128)}) custom-call(bf16[64,4,1024]{2,1,0:T(4,128)(2,1)S(1)} %get-tuple-element.4.tokens, f32[2,16,64,1024]{3,2,1,0:T(8,128)S(1)} %get-tuple-element.5.new), custom_call_target="tpu_custom_call" | custom-call | tf_op jit(solution)/shard_map/store/pallas_call | solution.py:819

commit v5 on v4

--- a/solution.py
+++ b/solution.py
@@ -53,7 +53,7 @@
     c.groups = c.own_seqs // c.per_tile
     c.parts = 8
     c.pairs = c.parts // 2
-    c.direct = 5 if m == 4 else 0
+    c.direct = 3 if m == 4 else 0
     c.part = c.feat // c.parts
     c.lanes = -(-c.seqs // 128) * 128
     return c
@@ -89,7 +89,11 @@
         return remote(full.at[p], full.at[p], full_s, full_r.at[p], "tp", away)
 
     def early(p):
-        return remote(sent.at[p], came.at[p], in_s, early_r.at[p - straight], "tp", away)
+        return remote(sent.at[p], came.at[p], in_s, early_r, "tp", away)
+
+    def early_all():
+        some = sent.at[pl.ds(0, direct)]
+        return remote(some, some, in_s, early_r, "tp", away)
 
     def jump(p):
         far = 2 * toward - z
@@ -138,7 +142,8 @@
 
             @pl.when(depth == 0)
             def _():
-                early(p).wait_recv()
+                if p == straight:
+                    early_all().wait_recv()
                 mid[p] = (sent[p].astype(F32) + came[p].astype(F32)).astype(BF16)
                 jump(p).wait_recv()
                 full[p] = (mid[p].astype(F32) + over[p].astype(F32)).astype(BF16)
@@ -291,16 +296,18 @@
         s.raw_small[1] = jnp.broadcast_to(squares, (c.rows, ab)).astype(BF16)
         raw_swap(-1).start()
 
+    raws = min(2, c.chunks)
+
     def raw_swap(j):
-        x, pair = (s.raw_small, s.raw_pair_small) if j < 0 else (s.raw, s.raw_pair)
+        x, pair = (s.raw_small, s.raw_pair_small) if j < 0 else (s.raw.at[j], s.raw_pair.at[j])
         return remote(x.at[1 - core], pair, s.raw_s.at[j + 1], s.first_r.at[j + 1], "dp", partner)
 
-    def raw_first():
-        wait_weights(0, 0)
-        val = dot(s.bent[...], s.w[0, 0]).astype(BF16)
-        s.raw[0] = val[:, : 2 * tile]
-        s.raw[1] = val[:, 2 * tile :]
-        raw_swap(0).start()
+    def raw_first(j):
+        wait_weights(0, j)
+        val = dot(s.bent[...], s.w[0, j]).astype(BF16)
+        s.raw[j, 0] = val[:, : 2 * tile]
+        s.raw[j, 1] = val[:, 2 * tile :]
+        raw_swap(j).start()
 
     def wait_counts():
         every = s.counts.at[pl.ds(0, n - 1)]
@@ -308,7 +315,7 @@
         swap.wait()
 
     def raw_cross(j):
-        x, pair = (s.raw_small, s.raw_pair_small) if j < 0 else (s.raw, s.raw_pair)
+        x, pair = (s.raw_small, s.raw_pair_small) if j < 0 else (s.raw.at[j], s.raw_pair.at[j])
         raw_swap(j).wait_recv()
         total = (x[core].astype(F32) + pair[...].astype(F32)).astype(BF16)
         bufs(0, j)[2][...] = dot(s.into[...], total).astype(BF16)
@@ -316,7 +323,8 @@
             second(0, j, d).start()
 
     raw_small()
-    raw_first()
+    for j in range(raws):
+        raw_first(j)
     load_rest(0)
     wait_counts()
     total = s.counts[0]
@@ -522,10 +530,10 @@
         if l:
             first(l, -1).wait_send()
         else:
-            for j in (-1, 0):
+            for j in range(-1, raws):
                 raw_swap(j).wait_send()
-        if l or c.chunks > 1:
-            done = s.pair.at[l] if l else s.pair.at[l, pl.ds(1, c.chunks - 1)]
+        if l or c.chunks > raws:
+            done = s.pair.at[l] if l else s.pair.at[l, pl.ds(raws, c.chunks - raws)]
             remote(done, done, s.first_s.at[1], s.first_r.at[0], "dp", partner).wait_send()
         for d in range(chips - 1):
             second(l, -1, d).wait_send()
@@ -561,11 +569,18 @@
         for i in range(per):
             lines[l].start(run * per + i)
 
+    lead = 5
+    early_takes = c.parts - lead if c.direct else 0
+    early_takes = min(early_takes, c.parts - c.direct)
+
     def mix_out(l, p):
         lines[l].relay(p)
+        if 0 <= p - lead < early_takes:
+            lines[l].take(p - lead)
 
     def mix_in(l, p):
-        lines[l].take(p)
+        if not p < early_takes:
+            lines[l].take(p)
         at = slice(p * c.part, (p + 1) * c.part)
         mixed = (s.h[:, at] + s.full[l, p].astype(F32)).astype(BF16)
         s.scaled[:, at] = mixed
@@ -646,30 +661,34 @@
                     s.acc_small[...] = val if p == 1 else s.acc_small[...] + val
         if l:
             produce_small(l)
-            produce(l, 0)
+            for j in range(c.chunks):
+                produce(l, j)
+                if j:
+                    cross(l, j - 2)
+            for j in range(c.chunks - 2, c.chunks):
+                cross(l, j)
         else:
-            raw_cross(-1)
-            raw_cross(0)
+            for j in range(-1, raws):
+                raw_cross(j)
             pack_rest()
-        for j in range(1, c.chunks):
-            produce(l, j)
-            if l:
-                cross(l, j - 2)
-            elif j > 1:
-                cross(l, j - 1)
-        if l:
-            cross(l, c.chunks - 2)
-        if l or c.chunks > 1:
-            cross(l, c.chunks - 1)
+            for j in range(raws, c.chunks):
+                produce(l, j)
+            for copy in late:
+                copy.wait()
+            setup()
+            round_states(0)
+            for j in range(raws, c.chunks):
+                if j + 1 == c.chunks:
+                    finish(l, -1)
+                cross(l, j)
+            if c.chunks == raws:
+                finish(l, -1)
         if l == 0:
             for j in range(c.chunks):
                 load_weights(1, j)
             load_rest(1)
-            for copy in late:
-                copy.wait()
-            setup()
-            round_states(0)
-        finish(l, -1)
+        else:
+            finish(l, -1)
         finish(l, 0)
         prepare(l)
         for j in range(1, c.chunks):
@@ -723,9 +742,9 @@
         channel=buf(BLOCKS, c.size),
         shrink=wide(BLOCKS, c.own_seqs, c.slots, c.heads),
         w=buf(BLOCKS, c.chunks, c.feat, 4 * c.tile),
-        raw=buf(2, c.rows, half),
+        raw=buf(min(2, c.chunks), 2, c.rows, half),
         raw_small=buf(2, c.rows, ab),
-        raw_pair=buf(c.rows, half),
+        raw_pair=buf(min(2, c.chunks), c.rows, half),
         raw_pair_small=buf(c.rows, ab),
         hot=buf(c.rows, c.packed),
         alive=wide(c.rows, 128),
@@ -769,7 +788,7 @@
         wo_sem=dma(BLOCKS),
         state_sem=dma(BLOCKS),
         count_sem=dma(2),
-        raw_s=dma(2),
+        raw_s=dma(1 + min(2, c.chunks)),
         first_s=dma(2),
         first_r=dma(every),
         second_s=dma(2, chips - 1),
@@ -779,9 +798,9 @@
         y_s=dma(1),
         y_r=dma(2),
         line_s=dma(4),
-        early_r=dma(BLOCKS, max(c.direct, 1)),
+        early_r=dma(BLOCKS),
         in_r=dma(c.parts),
-        full_r=dma(c.parts),
+        full_r=dma(c.parts - c.direct),
         over_r=dma(BLOCKS, c.parts),
     )
     c.names = list(scratch)

time: 65.8 us -> 65.4 us (level)
  no operation moved by 1% of the time
where the time goes in v5:
time: 65.4 us; the launch traced here: 65.2 us
  Pallas kernels  64.4 us (98%)
  between operations  0.8 us (1%)
    pallas_call x1, Pallas kernels, run_main(): pl.pallas_call(functools.partial(main_kernel, c), out_shape=[pltpu.VMEM(a...  60.8 us
    pallas_call x1, Pallas kernels, store(): pl.pallas_call(functools.partial(store_kernel, pieces), out_shape=[jax.Sh...  3.55 us

profile of v5, /device:TPU:0, one launch (start us, length us, event | category | flops | bytes accessed | tf_op | source)
XLA Modules:
  0.0 65.2 jit_solution(5457903795034105575)
XLA Ops:
  0.6 60.8 %blocks.1 = (bf16[64,4,1024]{2,1,0:T(4,128)(2,1)S(1)}, f32[2,16,64,1024]{3,2,1,0:T(8,128)S(1)}) custom-call(s32[16]{0:T(128)} %counts.1, bf16[64,4,1024]{2,1,0:T(4,128)(2,1)} %resid.1, bf16[2,1024,1024]{2,1,0:T(8,128)(2,1)} %wq.1, bf16[2,1024,1024]{2,1,0:T(8,128)(2,1)} %wk.1, bf16[2,1024,1024]{2,1,0:T(8,128)(2,1)} %wv.1, bf16[2,1024,1024]{2,1,0:T(8,128)(2,1)} %wz.1, ...), custom_call_target="tpu_custom_call" | custom-call | tf_op jit(solution)/shard_map/blocks/pallas_call | solution.py:807
  61.5 3.5 %store.1 = (bf16[64,4,1024]{2,1,0:T(4,128)(2,1)}, f32[2,16,64,1024]{3,2,1,0:T(8,128)}) custom-call(bf16[64,4,1024]{2,1,0:T(4,128)(2,1)S(1)} %get-tuple-element.4.tokens, f32[2,16,64,1024]{3,2,1,0:T(8,128)S(1)} %get-tuple-element.5.new), custom_call_target="tpu_custom_call" | custom-call | tf_op jit(solution)/shard_map/store/pallas_call | solution.py:838

commit v6 on v5

--- a/solution.py
+++ b/solution.py
@@ -275,10 +275,8 @@
         row = lax.div(iota((tile, tile), 0), c.size)
         col = lax.div(iota((tile, tile), 1), c.size)
         s.blocks[...] = (row == col).astype(BF16)
-        for g in range(c.groups):
-            r = lax.rem(iota((2 * c.own, tile), 0), c.own_seqs)
-            k = g * c.per_tile + lax.div(iota((2 * c.own, tile), 1), c.size)
-            s.mask[g] = (r == k).astype(BF16)
+        shape = s.mask.shape
+        s.mask[...] = (lax.rem(iota(shape, 0), c.per_tile) == lax.div(iota(shape, 1), c.size)).astype(BF16)
 
     for j in range(1, c.chunks):
         load_weights(0, j)
@@ -431,10 +429,11 @@
         third(l, -1).wait_recv()
         pick = s.pick[...]
         heads = c.heads
-        few = dot(pick, s.fin_small[l, 0]).astype(BF16)
+        few = dot(pick[: c.own], s.fin_small[l, 0]).astype(BF16)
         squares = dot(pick, s.fin_small[l, 1])[:, :1]
         factor = lax.rsqrt(squares / (c.feat * n) + EPS)
         s.factor[...] = jnp.broadcast_to(factor, s.factor.shape)
+        factor = factor[: c.own]
         at = iota((ab, heads), 1) + z * heads
         pa = dot(few, (iota((ab, heads), 0) == at).astype(BF16)) * factor
         pb = dot(few, (iota((ab, heads), 0) == at + all_heads).astype(BF16)) * factor
@@ -457,23 +456,36 @@
         pick = s.pick[...]
         factor = s.factor[:, :1]
         qk = dot(pick, s.fin[l, j, 0]) * factor
-        vz = dot(pick, s.fin[l, j, 1]) * factor
+        vz = dot(pick[: c.own], s.fin[l, j, 1]) * factor[: c.own]
         qk = qk * jax.nn.sigmoid(qk)
         vz = vz * jax.nn.sigmoid(vz)
-        q, k = qk[:, :tile], qk[:, tile:]
+        q, k = qk[: c.own, :tile], qk[: c.own, tile:]
         v, zed = vz[:, :tile], vz[:, tile:]
-        both = jnp.concatenate([k, q], axis=0)
+        both = jnp.concatenate([qk[c.own :, tile:], qk[c.own :, :tile]], axis=0)
         low = iota((2 * c.own, 128), 1) < c.size
         copies = []
         for i in range(tile // 128):
             here = both[:, i * 128 : (i + 1) * 128]
             turned = pltpu.roll(here, c.size, 1)
             copies += [jnp.where(low, here, turned), jnp.where(low, turned, here)]
-        lhs = []
-        for one in copies:
-            wide = jnp.concatenate([one.astype(BF16)] * (tile // 128), axis=1)
-            lhs.append(jnp.concatenate([wide * s.mask[g] for g in range(c.groups)], axis=1))
-        read = dot(jnp.concatenate(lhs, axis=0), s.states16[l, :, at])
+        heads = [jnp.concatenate([one.astype(BF16)] * (tile // 128), axis=1) for one in copies]
+        batch = c.slots * c.per_tile
+        lane_head = lax.div(iota((2 * batch, tile), 1), c.size)
+        reads = []
+        for g in range(c.groups):
+            rows = [
+                wide[start + g * batch : start + (g + 1) * batch] for wide in heads for start in (0, c.own)
+            ]
+            read = dot(jnp.concatenate(rows, axis=0) * s.mask[...], s.states16[l, g * tile : (g + 1) * tile, at])
+            kept = read[: 2 * batch]
+            for h in range(1, c.per_tile):
+                kept = jnp.where(lane_head == h, read[2 * batch * h : 2 * batch * (h + 1)], kept)
+            reads.append(kept)
+
+        def read_step(first, t):
+            rows = slice(first + t * c.per_tile, first + (t + 1) * c.per_tile)
+            return jnp.concatenate([kept[rows] for kept in reads], axis=0)
+
         step = lambda x, t: x[t * c.own_seqs : (t + 1) * c.own_seqs]
         names, prods = [], []
         for t in range(c.slots):
@@ -489,12 +501,6 @@
         nk = [lax.rsqrt(pairs["k", t, t] + EPS) for t in range(c.slots)]
         nq = [lax.rsqrt(pairs["n", t, t] + EPS) * c.size ** (-0.5) for t in range(c.slots)]
         s.k[l, :, at] = (k * jnp.concatenate(nk, axis=0)).astype(BF16)
-        lane_head = lax.div(iota((2 * c.own, tile), 1), c.size)
-        reads = read[: 2 * c.own]
-        for h in range(1, c.per_tile):
-            reads = jnp.where(lane_head == h, read[2 * c.own * h : 2 * c.own * (h + 1)], reads)
-        rk = reads[: c.own]
-        rq = reads[c.own :]
         dec = s.dec[:, at]
         beta = s.beta[:, at]
         fresh, outs = [], []
@@ -503,11 +509,11 @@
             g = step(dec, t)
             whole = g if whole is None else whole * g
             fresh = [(u * g) for u in fresh]
-            guess = whole * step(rk, t)
+            guess = whole * read_step(0, t)
             for i in range(t):
                 guess = guess + pairs["k", i, t] * nk[i] * fresh[i]
             fresh.append(step(beta, t) * (step(v, t) - guess * nk[t]))
-            o = whole * step(rq, t)
+            o = whole * read_step(batch, t)
             for i in range(t + 1):
                 o = o + pairs["q", i, t] * nk[i] * fresh[i]
             outs.append(o * nq[t])
@@ -597,11 +603,15 @@
         tokens[:, :, at] = mixed.reshape(c.seqs, c.slots, 2 * c.part)
 
     def setup():
-        r = iota((c.own, c.lanes), 0)
-        pos, live = columns(c.own, lax.rem(r, c.own_seqs) + me * c.own_seqs, lax.div(r, c.own_seqs))
-        offset = (iota((c.own, c.win), 1) + me * c.own_seqs).astype(F32)
+        r = iota((2 * c.own, c.lanes), 0)
+        again = r - c.own
+        few = lax.rem(again, c.per_tile) + lax.div(again, c.slots * c.per_tile) * c.per_tile
+        seq = jnp.where(r < c.own, lax.rem(r, c.own_seqs), few)
+        slot = jnp.where(r < c.own, lax.div(r, c.own_seqs), lax.rem(lax.div(again, c.per_tile), c.slots))
+        pos, live = columns(2 * c.own, seq + me * c.own_seqs, slot)
+        offset = (iota((2 * c.own, c.win), 1) + me * c.own_seqs).astype(F32)
         s.pick[...] = jnp.where((offset == pos) & live, 1.0, 0.0).astype(BF16)
-        s.live[...] = jnp.broadcast_to(jnp.where(live, 1.0, 0.0), s.live.shape)
+        s.live[...] = jnp.broadcast_to(jnp.where(live, 1.0, 0.0)[: c.own], s.live.shape)
         shape = (c.lanes, c.own)
         pos, live = rows_of(
             lax.rem(iota(shape, 1), c.own_seqs) + me * c.own_seqs, lax.div(iota(shape, 1), c.own_seqs)
@@ -755,12 +765,12 @@
         states16=buf(BLOCKS, c.own_seqs * c.size, c.cols),
         counts=pltpu.VMEM((n, 8, c.lanes), jnp.int32),
         blocks=buf(c.tile, c.tile),
-        mask=buf(c.groups, 2 * c.own, c.tile),
+        mask=buf(c.per_tile * 2 * c.slots * c.per_tile, c.tile),
         gain=wide(BLOCKS, 8, c.tile),
-        pick=buf(c.own, c.win),
+        pick=buf(2 * c.own, c.win),
         place=buf(c.win, c.own),
         live=wide(c.own, 128),
-        factor=wide(c.own, 128),
+        factor=wide(2 * c.own, 128),
         dec=wide(c.own, c.cols),
         beta=wide(c.own, c.cols),
         h=wide(c.packed, c.feat),

time: 65.4 us -> 64.4 us (0.985)
  Pallas kernels: 64.4 us -> 63.5 us
    pallas_call x1, Pallas kernels: 60.8 us -> 59.9 us  [run_main(): pl.pallas_call(functools.partial(main_kernel, c), out_shape=[pltpu.VMEM(a...]
where the time goes in v6:
time: 64.4 us; the launch traced here: 64.3 us
  Pallas kernels  63.5 us (99%)
  between operations  0.8 us (1%)
    pallas_call x1, Pallas kernels, run_main(): pl.pallas_call(functools.partial(main_kernel, c), out_shape=[pltpu.VMEM(a...  59.9 us
    pallas_call x1, Pallas kernels, store(): pl.pallas_call(functools.partial(store_kernel, pieces), out_shape=[jax.Sh...  3.55 us

profile of v6, /device:TPU:0, one launch (start us, length us, event | category | flops | bytes accessed | tf_op | source)
XLA Modules:
  0.0 64.3 jit_solution(17427531918842237329)
XLA Ops:
  0.6 59.9 %blocks.1 = (bf16[64,4,1024]{2,1,0:T(4,128)(2,1)S(1)}, f32[2,16,64,1024]{3,2,1,0:T(8,128)S(1)}) custom-call(s32[16]{0:T(128)} %counts.1, bf16[64,4,1024]{2,1,0:T(4,128)(2,1)} %resid.1, bf16[2,1024,1024]{2,1,0:T(8,128)(2,1)} %wq.1, bf16[2,1024,1024]{2,1,0:T(8,128)(2,1)} %wk.1, bf16[2,1024,1024]{2,1,0:T(8,128)(2,1)} %wv.1, bf16[2,1024,1024]{2,1,0:T(8,128)(2,1)} %wz.1, ...), custom_call_target="tpu_custom_call" | custom-call | tf_op jit(solution)/shard_map/blocks/pallas_call | solution.py:817
  60.6 3.5 %store.1 = (bf16[64,4,1024]{2,1,0:T(4,128)(2,1)}, f32[2,16,64,1024]{3,2,1,0:T(8,128)}) custom-call(bf16[64,4,1024]{2,1,0:T(4,128)(2,1)S(1)} %get-tuple-element.4.tokens, f32[2,16,64,1024]{3,2,1,0:T(8,128)S(1)} %get-tuple-element.5.new), custom_call_target="tpu_custom_call" | custom-call | tf_op jit(solution)/shard_map/store/pallas_call | solution.py:848
